TPU v7x, 32 devices: a whole 2x2x4 slice. The times are simulated.
32 devices in a mesh: sp: 8 (over z, x), tp: 4 (over y, core).
Axes of the slice: x: 2, y: 2, z: 4, core: 2. Of those that a mesh axis runs over, the one named last changes fastest.
Arguments:
- stream: bfloat16 [4096, 2048], P(('sp', 'tp')), may hold values from -6 to 6
- queries: bfloat16 [4096, 512], P('sp', 'tp'), may hold values from -6 to 6
- key_rows: bfloat16 [4096, 512], P('sp', 'tp'), may hold values from -6 to 6
- values: bfloat16 [4096, 1024], P('sp', 'tp'), may hold values from -6 to 6
- out_gate: bfloat16 [4096, 1024], P('sp', 'tp'), may hold values from -6 to 6
- fwd_decay: float32 [4096, 512], P('sp', 'tp'), may hold values from -14 to 14
- bwd_decay: float32 [4096, 512], P('sp', 'tp'), may hold values from -14 to 14
- head_gain: float32 [1024], P('tp'), may hold values from 0.1 to 1.9
- out_proj: bfloat16 [1024, 2048], replicated, may hold values from -0.1875 to 0.1875
- mix_gain: float32 [2048], replicated, may hold values from 0.1 to 1.9
- ffn_gain: float32 [2048], replicated, may hold values from 0.1 to 1.9
- moe_gain: float32 [2048], replicated, may hold values from 0.1 to 1.9
- routes: int32 [4096, 2], P(('sp', 'tp')), may hold values from 0 to 7, all different within a row; in each aligned block of 128 rows (0 to 127, 128 to 255, ...) at most 48 rows name the same one
- route_weight: float32 [4096, 2], P(('sp', 'tp')), may hold values from 0.25 to 2.5
- expert_gate: bfloat16 [8, 2048, 1024], P('sp', None, 'tp'), may hold values from -0.125 to 0.125
- expert_up: bfloat16 [8, 2048, 1024], P('sp', None, 'tp'), may hold values from -0.125 to 0.125
- expert_down: bfloat16 [8, 1024, 2048], P('sp', 'tp'), may hold values from -0.1875 to 0.1875
- shared_gate: bfloat16 [2048, 512], P(None, 'tp'), may hold values from -0.125 to 0.125
- shared_up: bfloat16 [2048, 512], P(None, 'tp'), may hold values from -0.125 to 0.125
- shared_down: bfloat16 [512, 2048], P('tp'), may hold values from -0.25 to 0.25
Outputs:
- updated: bfloat16 [4096, 2048], P(('sp', 'tp'))
Inputs may be any that keep to these rules, and one draw needn't show every extreme that they name: `routes`: each row names 2 different experts. Among the rows of one device no expert is named more than 48 times, and in every draw some device names some expert exactly 48 times.
All inputs are finite; a program needn't handle non-finite values.
Results may differ from a plain program's by a relative error of at most 0.023.
Values may be sent and summed in bfloat16 or wider, within the bound.
A program may use at most 128 MiB of HBM per device.

v0:
```python
import functools

import jax
import jax.numpy as jnp
from jax import lax
from jax.experimental import pallas as pl
from jax.experimental.pallas import tpu as pltpu
from jax.sharding import PartitionSpec as P

KEY_CHANNELS = 64
DV = 128
BLK = 64
TOPK = 2


EPS = 1e-06
GATE_NORM = 16.0
ROPE_BASE = 10000.0
TOP_PRECISION = lax.Precision.HIGHEST
MESH = pl.DeviceIdType.MESH


def normalize(tensor):
    return tensor * lax.rsqrt(jnp.mean(tensor * tensor, axis=-1, keepdims=True) + EPS)


def dot_nt(left, right):
    return lax.dot_general(
        left, right, (((1,), (1,)), ((), ())), preferred_element_type=jnp.float32
    )


def dot_tn(left, right):
    return lax.dot_general(
        left, right, (((0,), (0,)), ((), ())), preferred_element_type=jnp.float32
    )


def attention_kernel(
    sp_count,
    tp_count,
    q_ref,
    k_ref,
    v_ref,
    gate_ref,
    fwd_ref,
    bwd_ref,
    cos_ref,
    sin_ref,
    gain_ref,
    out_ref,
    own_ref,
    got_ref,
    mixed_ref,
    land_ref,
    within_ref,
    key_ref,
    sums_f,
    sums_b,
    sum_send,
    sum_recv,
    row_send,
    row_recv,
):
    span, lanes = q_ref.shape
    width = v_ref.shape[1]
    heads = lanes // KEY_CHANNELS
    blocks = span // BLK
    rows_out = span // tp_count
    sp_me = lax.axis_index("sp")
    tp_me = lax.axis_index("tp")

    barrier = pltpu.get_barrier_semaphore()
    for step in range(1, sp_count):
        pl.semaphore_signal(
            barrier,
            inc=1,
            device_id=(lax.rem(sp_me + step, sp_count), tp_me),
            device_id_type=MESH,
        )
    for step in range(1, tp_count):
        pl.semaphore_signal(
            barrier,
            inc=1,
            device_id=(sp_me, lax.rem(tp_me + step, tp_count)),
            device_id_type=MESH,
        )

    row = lax.broadcasted_iota(jnp.int32, (BLK, BLK), 0)
    column = lax.broadcasted_iota(jnp.int32, (BLK, BLK), 1)
    lower = row >= column
    upper = row <= column
    lower_ones = lower.astype(jnp.float32)
    upper_ones = upper.astype(jnp.float32)
    from_lane = lax.broadcasted_iota(jnp.int32, (lanes, lanes), 0)
    to_lane = lax.broadcasted_iota(jnp.int32, (lanes, lanes), 1)
    half = KEY_CHANNELS // 2
    partner = jnp.where(lax.rem(to_lane, KEY_CHANNELS) < half, to_lane + half, to_lane - half)
    swap = (from_lane == partner).astype(jnp.bfloat16)
    own_head = (
        lax.broadcasted_iota(jnp.int32, (width, lanes), 0) // DV
        == lax.broadcasted_iota(jnp.int32, (width, lanes), 1) // KEY_CHANNELS
    )
    lane_head = lax.broadcasted_iota(jnp.int32, (BLK, lanes), 1) // KEY_CHANNELS

    def rotated(tensor, rows):
        swapped = jnp.dot(tensor, swap, preferred_element_type=jnp.float32)
        return tensor.astype(jnp.float32) * cos_ref[rows, :] + swapped * sin_ref[rows, :]

    cumul_f, cumul_b, decay_f, decay_b = [], [], [], []
    for block in range(blocks):
        rows = pl.ds(block * BLK, BLK)
        total_f = jnp.dot(
            lower_ones, fwd_ref[rows, :], precision=TOP_PRECISION, preferred_element_type=jnp.float32
        )
        total_b = jnp.dot(
            upper_ones, bwd_ref[rows, :], precision=TOP_PRECISION, preferred_element_type=jnp.float32
        )
        last_f = total_f[BLK - 1 : BLK]
        last_b = total_b[0:1]
        keys = rotated(k_ref[rows, :], rows)
        key_ref[rows, :] = keys
        value_rows = v_ref[rows, :]
        out_f = (keys * jnp.exp(last_f - total_f)).astype(jnp.bfloat16)
        out_b = (keys * jnp.exp(last_b - total_b)).astype(jnp.bfloat16)
        sums_f[block] = jnp.where(own_head, dot_tn(value_rows, out_f), 0.0)
        sums_b[block] = jnp.where(own_head, dot_tn(value_rows, out_b), 0.0)
        cumul_f.append(total_f)
        cumul_b.append(total_b)
        decay_f.append(jnp.exp(last_f))
        decay_b.append(jnp.exp(last_b))

    def packed(total):
        return sum(total[h * DV : (h + 1) * DV] for h in range(heads))

    total = sums_f[0]
    through = decay_f[0]
    for block in range(1, blocks):
        total = total * decay_f[block] + sums_f[block]
        through = through * decay_f[block]
    own_ref[0:DV, :] = packed(total).astype(jnp.bfloat16)
    own_ref[2 * DV : 2 * DV + 8, :] = jnp.broadcast_to(through, (8, lanes)).astype(jnp.bfloat16)
    total = sums_b[blocks - 1]
    through = decay_b[blocks - 1]
    for block in range(blocks - 2, -1, -1):
        total = total * decay_b[block] + sums_b[block]
        through = through * decay_b[block]
    own_ref[DV : 2 * DV, :] = packed(total).astype(jnp.bfloat16)
    own_ref[2 * DV + 8 : 2 * DV + 16, :] = jnp.broadcast_to(through, (8, lanes)).astype(
        jnp.bfloat16
    )

    pl.semaphore_wait(barrier, sp_count - 1 + tp_count - 1)
    sum_copies = []
    for step in range(1, sp_count):
        copy = pltpu.make_async_remote_copy(
            src_ref=own_ref,
            dst_ref=got_ref.at[step],
            send_sem=sum_send.at[step],
            recv_sem=sum_recv.at[step],
            device_id=(lax.rem(sp_me + step, sp_count), tp_me),
            device_id_type=MESH,
        )
        copy.start()
        sum_copies.append(copy)

    query_f, query_b = [], []
    for block in range(blocks):
        rows = pl.ds(block * BLK, BLK)
        queries = rotated(q_ref[rows, :], rows) * KEY_CHANNELS ** (-0.5)
        keys = key_ref[rows, :]
        total_f, total_b = cumul_f[block], cumul_b[block]
        middle_f = total_f[BLK // 2 - 1 : BLK // 2]
        middle_b = total_b[BLK // 2 : BLK // 2 + 1]
        scaled_qf = queries * jnp.exp(total_f - middle_f)
        scaled_qb = queries * jnp.exp(total_b - middle_b)
        scaled_kf = (keys * jnp.exp(middle_f - total_f)).astype(jnp.bfloat16)
        scaled_kb = (keys * jnp.exp(middle_b - total_b)).astype(jnp.bfloat16)
        query_f.append((queries * jnp.exp(total_f)).astype(jnp.bfloat16))
        query_b.append((queries * jnp.exp(total_b)).astype(jnp.bfloat16))
        for h in range(heads):
            mine = lane_head == h
            scores_f = dot_nt(jnp.where(mine, scaled_qf, 0.0).astype(jnp.bfloat16), scaled_kf)
            scores_b = dot_nt(jnp.where(mine, scaled_qb, 0.0).astype(jnp.bfloat16), scaled_kb)
            scores = jnp.where(lower, scores_f, 0.0) + jnp.where(upper, scores_b, 0.0)
            within_ref[rows, h * DV : (h + 1) * DV] = jnp.dot(
                scores.astype(jnp.bfloat16),
                v_ref[rows, h * DV : (h + 1) * DV],
                preferred_element_type=jnp.float32,
            )

    for copy in sum_copies:
        copy.wait()
    carry_f = jnp.zeros((DV, lanes), jnp.float32)
    carry_b = jnp.zeros((DV, lanes), jnp.float32)
    for step in range(sp_count - 1, 0, -1):
        state = got_ref[step, 0:DV, :].astype(jnp.float32)
        through = got_ref[step, 2 * DV : 2 * DV + 16, :].astype(jnp.float32)[0:1]
        carry_f = jnp.where(step <= sp_me, carry_f * through + state, carry_f)
    for step in range(1, sp_count):
        state = got_ref[step, DV : 2 * DV, :].astype(jnp.float32)
        through = got_ref[step, 2 * DV : 2 * DV + 16, :].astype(jnp.float32)[8:9]
        carry_b = jnp.where(step > sp_me, carry_b * through + state, carry_b)

    def unpacked(carry):
        return jnp.where(own_head, jnp.concatenate([carry] * heads, axis=0), 0.0)

    state = unpacked(carry_f)
    for block in range(blocks):
        rows = pl.ds(block * BLK, BLK)
        within_ref[rows, :] += dot_nt(query_f[block], state.astype(jnp.bfloat16))
        if block < blocks - 1:
            state = state * decay_f[block] + sums_f[block]
    state = unpacked(carry_b)
    for block in range(blocks - 1, -1, -1):
        rows = pl.ds(block * BLK, BLK)
        attended = within_ref[rows, :] + dot_nt(query_b[block], state.astype(jnp.bfloat16))
        if block > 0:
            state = state * decay_b[block] + sums_b[block]
        for h in range(heads):
            part = attended[:, h * DV : (h + 1) * DV]
            square = jnp.mean(part * part, axis=-1, keepdims=True)
            gate = gate_ref[rows, h * DV : (h + 1) * DV].astype(jnp.float32)
            mixed_ref[rows, h * DV : (h + 1) * DV] = (
                part
                * lax.rsqrt(square + EPS)
                * gain_ref[:, h * DV : (h + 1) * DV]
                * (gate / (1.0 + jnp.exp(-gate)))
            ).astype(jnp.bfloat16)

    row_copies = []
    for step in range(1, tp_count):
        target = lax.rem(tp_me + step, tp_count)
        copy = pltpu.make_async_remote_copy(
            src_ref=mixed_ref.at[pl.ds(pl.multiple_of(target * rows_out, rows_out), rows_out)],
            dst_ref=land_ref.at[tp_me],
            send_sem=row_send.at[step],
            recv_sem=row_recv.at[step],
            device_id=(sp_me, target),
            device_id_type=MESH,
        )
        copy.start()
        row_copies.append(copy)
    land_ref[tp_me] = mixed_ref[pl.ds(pl.multiple_of(tp_me * rows_out, rows_out), rows_out), :]
    for copy in row_copies:
        copy.wait()
    for source in range(tp_count):
        out_ref[:, source * width : (source + 1) * width] = land_ref[source]


def attention(queries, key_rows, values, out_gate, fwd_log, bwd_log, cosine, signed_sine, gain):
    sp_count = lax.axis_size("sp")
    tp_count = lax.axis_size("tp")
    span, lanes = queries.shape
    width = values.shape[1]
    rows_out = span // tp_count
    blocks = span // BLK
    vmem = pl.BlockSpec(memory_space=pltpu.VMEM)
    return pl.pallas_call(
        functools.partial(attention_kernel, sp_count, tp_count),
        out_shape=jax.ShapeDtypeStruct((rows_out, tp_count * width), jnp.bfloat16),
        in_specs=[vmem] * 9,
        out_specs=vmem,
        scratch_shapes=[
            pltpu.VMEM((2 * DV + 16, lanes), jnp.bfloat16),
            pltpu.VMEM((sp_count, 2 * DV + 16, lanes), jnp.bfloat16),
            pltpu.VMEM((span, width), jnp.bfloat16),
            pltpu.VMEM((tp_count, rows_out, width), jnp.bfloat16),
            pltpu.VMEM((span, width), jnp.float32),
            pltpu.VMEM((span, lanes), jnp.float32),
            pltpu.VMEM((blocks, width, lanes), jnp.float32),
            pltpu.VMEM((blocks, width, lanes), jnp.float32),
            pltpu.SemaphoreType.DMA((sp_count,)),
            pltpu.SemaphoreType.DMA((sp_count,)),
            pltpu.SemaphoreType.DMA((tp_count,)),
            pltpu.SemaphoreType.DMA((tp_count,)),
        ],
        compiler_params=pltpu.CompilerParams(collective_id=0, has_side_effects=True),
    )(queries, key_rows, values, out_gate, fwd_log, bwd_log, cosine, signed_sine, gain)


def dispatch_kernel(
    sp_count,
    tp_count,
    outgoing_ref,
    rows_ref,
    gate_ref,
    up_ref,
    down_ref,
    arrived_ref,
    shared_ref,
    part_ref,
    block_land,
    row_land,
    block_send,
    block_recv,
    row_send,
    row_recv,
):
    sp_me = lax.axis_index("sp")
    tp_me = lax.axis_index("tp")

    def sp_peer(step):
        return (lax.rem(sp_me + step, sp_count), tp_me)

    def tp_peer(step):
        return (sp_me, lax.rem(tp_me + step, tp_count))

    barrier = pltpu.get_barrier_semaphore()
    for step in range(1, sp_count):
        pl.semaphore_signal(barrier, inc=1, device_id=sp_peer(step), device_id_type=MESH)
    for step in range(1, tp_count):
        pl.semaphore_signal(barrier, inc=1, device_id=tp_peer(step), device_id_type=MESH)
    pl.semaphore_wait(barrier, sp_count - 1 + tp_count - 1)

    row_copies, block_copies = [], []
    for step in range(1, tp_count):
        copy = pltpu.make_async_remote_copy(
            src_ref=rows_ref,
            dst_ref=row_land.at[step],
            send_sem=row_send.at[step],
            recv_sem=row_recv.at[step],
            device_id=tp_peer(step),
            device_id_type=MESH,
        )
        copy.start()
        row_copies.append(copy)
    for step in range(1, sp_count):
        copy = pltpu.make_async_remote_copy(
            src_ref=outgoing_ref.at[lax.rem(sp_me + step, sp_count)],
            dst_ref=block_land.at[sp_me],
            send_sem=block_send.at[step],
            recv_sem=block_recv.at[step],
            device_id=sp_peer(step),
            device_id_type=MESH,
        )
        copy.start()
        block_copies.append(copy)
    block_land[sp_me] = outgoing_ref[sp_me]

    def partial(rows):
        hidden = jax.nn.silu(
            jnp.dot(rows, gate_ref[...], preferred_element_type=jnp.float32)
        ) * jnp.dot(rows, up_ref[...], preferred_element_type=jnp.float32)
        return jnp.dot(
            hidden.astype(jnp.bfloat16), down_ref[...], preferred_element_type=jnp.float32
        )

    shared_ref[...] = partial(rows_ref[...])
    for step in range(1, tp_count):
        row_copies[step - 1].wait()
        part_ref[step] = partial(row_land[step]).astype(jnp.bfloat16)
    part_ref[0] = jnp.zeros(part_ref.shape[1:], part_ref.dtype)
    for copy in block_copies:
        copy.wait()
    arrived_ref[...] = block_land[...]


def dispatch(outgoing, normed, shared_gate, shared_up, shared_down):
    sp_count = lax.axis_size("sp")
    tp_count = lax.axis_size("tp")
    vmem = pl.BlockSpec(memory_space=pltpu.VMEM)
    several = pltpu.VMEM((tp_count,) + normed.shape, normed.dtype)
    return pl.pallas_call(
        functools.partial(dispatch_kernel, sp_count, tp_count),
        out_shape=(
            jax.ShapeDtypeStruct(outgoing.shape, outgoing.dtype),
            jax.ShapeDtypeStruct(normed.shape, jnp.float32),
            jax.ShapeDtypeStruct((tp_count,) + normed.shape, normed.dtype),
        ),
        in_specs=[vmem] * 5,
        out_specs=(vmem, vmem, vmem),
        scratch_shapes=[
            pltpu.VMEM(outgoing.shape, outgoing.dtype),
            several,
            pltpu.SemaphoreType.DMA((sp_count,)),
            pltpu.SemaphoreType.DMA((sp_count,)),
            pltpu.SemaphoreType.DMA((tp_count,)),
            pltpu.SemaphoreType.DMA((tp_count,)),
        ],
        compiler_params=pltpu.CompilerParams(collective_id=1, has_side_effects=True),
    )(outgoing, normed, shared_gate, shared_up, shared_down)


def expert_kernel(
    sp_count,
    tp_count,
    rows_ref,
    gate_hbm,
    up_hbm,
    down_hbm,
    high_ref,
    low_ref,
    shared_ref,
    part_ref,
    residual_ref,
    gain_ref,
    out_ref,
    gate_ref,
    up_ref,
    down_ref,
    total_ref,
    done_ref,
    back_ref,
    part_land,
    weight_sem,
    send_sem,
    recv_sem,
    part_send,
    part_recv,
):
    sp_me = lax.axis_index("sp")
    tp_me = lax.axis_index("tp")
    groups, _, width = gate_ref.shape
    capacity = done_ref.shape[1]

    fetches = []
    for group in range(groups):
        cut = pl.ds(group * width, width)
        trio = (
            pltpu.make_async_copy(gate_hbm.at[group], gate_ref.at[group], weight_sem.at[0, group]),
            pltpu.make_async_copy(up_hbm.at[group], up_ref.at[group], weight_sem.at[1, group]),
            pltpu.make_async_copy(down_hbm.at[cut], down_ref.at[cut], weight_sem.at[2, group]),
        )
        for copy in trio:
            copy.start()
        fetches.append(trio)

    barrier = pltpu.get_barrier_semaphore()
    for step in range(1, sp_count):
        pl.semaphore_signal(
            barrier,
            inc=1,
            device_id=(lax.rem(sp_me + step, sp_count), tp_me),
            device_id_type=MESH,
        )

    for step in range(1, tp_count):
        pl.semaphore_signal(
            barrier,
            inc=1,
            device_id=(sp_me, lax.rem(tp_me + step, tp_count)),
            device_id_type=MESH,
        )
    pl.semaphore_wait(barrier, sp_count - 1 + tp_count - 1)
    part_copies = []
    for step in range(1, tp_count):
        copy = pltpu.make_async_remote_copy(
            src_ref=part_ref.at[step],
            dst_ref=part_land.at[step],
            send_sem=part_send.at[step],
            recv_sem=part_recv.at[step],
            device_id=(sp_me, lax.rem(tp_me + tp_count - step, tp_count)),
            device_id_type=MESH,
        )
        copy.start()
        part_copies.append(copy)

    for group in range(groups):
        for copy in fetches[group]:
            copy.wait()
        hidden = (
            jax.nn.silu(jnp.dot(rows_ref[...], gate_ref[group], preferred_element_type=jnp.float32))
            * jnp.dot(rows_ref[...], up_ref[group], preferred_element_type=jnp.float32)
        ).astype(jnp.bfloat16)
        piece = jnp.dot(
            hidden,
            down_ref[group * width : (group + 1) * width, :],
            preferred_element_type=jnp.float32,
        )
        if group == 0:
            total_ref[...] = piece
        else:
            total_ref[...] += piece
    for source in range(sp_count):
        done_ref[source] = total_ref[source * capacity : (source + 1) * capacity, :].astype(
            done_ref.dtype
        )

    copies = []
    for step in range(1, sp_count):
        target = lax.rem(sp_me + step, sp_count)
        copy = pltpu.make_async_remote_copy(
            src_ref=done_ref.at[target],
            dst_ref=back_ref.at[sp_me],
            send_sem=send_sem.at[step],
            recv_sem=recv_sem.at[step],
            device_id=(target, tp_me),
            device_id_type=MESH,
        )
        copy.start()
        copies.append(copy)
    back_ref[sp_me] = done_ref[sp_me]
    for copy in copies:
        copy.wait()

    mixture = shared_ref[...]
    for step in range(1, tp_count):
        part_copies[step - 1].wait()
        mixture = mixture + part_land[step].astype(jnp.float32)
    for expert in range(sp_count):
        mixture = mixture + jnp.dot(
            high_ref[expert], back_ref[expert], preferred_element_type=jnp.float32
        )
        mixture = mixture + jnp.dot(
            low_ref[expert], back_ref[expert], preferred_element_type=jnp.float32
        )
    square = jnp.mean(mixture * mixture, axis=-1, keepdims=True)
    out_ref[...] = (
        residual_ref[...].astype(jnp.float32)
        + mixture * lax.rsqrt(square + EPS) * gain_ref[...]
    ).astype(out_ref.dtype)


def run_expert(rows, gate_parts, up_parts, down_mat, high, low, shared_sum, parts, residual, gain):
    sp_count = lax.axis_size("sp")
    groups = gate_parts.shape[0]
    vmem = pl.BlockSpec(memory_space=pltpu.VMEM)
    hbm = pl.BlockSpec(memory_space=pl.ANY)
    blocked = pltpu.VMEM((sp_count, rows.shape[0] // sp_count, rows.shape[1]), rows.dtype)
    return pl.pallas_call(
        functools.partial(expert_kernel, sp_count, lax.axis_size("tp")),
        out_shape=jax.ShapeDtypeStruct(residual.shape, residual.dtype),
        in_specs=[vmem, hbm, hbm, hbm] + [vmem] * 6,
        out_specs=vmem,
        scratch_shapes=[
            pltpu.VMEM(gate_parts.shape, gate_parts.dtype),
            pltpu.VMEM(up_parts.shape, up_parts.dtype),
            pltpu.VMEM(down_mat.shape, down_mat.dtype),
            pltpu.VMEM(rows.shape, jnp.float32),
            blocked,
            blocked,
            pltpu.VMEM(parts.shape, parts.dtype),
            pltpu.SemaphoreType.DMA((3, groups)),
            pltpu.SemaphoreType.DMA((sp_count,)),
            pltpu.SemaphoreType.DMA((sp_count,)),
            pltpu.SemaphoreType.DMA((parts.shape[0],)),
            pltpu.SemaphoreType.DMA((parts.shape[0],)),
        ],
        compiler_params=pltpu.CompilerParams(collective_id=2, has_side_effects=True),
    )(rows, gate_parts, up_parts, down_mat, high, low, shared_sum, parts, residual, gain)


def slot_map(route_block, experts, capacity):
    tokens, choices = route_block.shape
    flat_ids = route_block.reshape(-1)
    total = flat_ids.shape[0]
    onehot = (flat_ids[:, None] == jnp.arange(experts, dtype=jnp.int32)[None, :]).astype(
        jnp.bfloat16
    )
    earlier = (jnp.arange(total)[:, None] > jnp.arange(total)[None, :]).astype(jnp.bfloat16)
    before = jnp.dot(earlier, onehot, preferred_element_type=jnp.float32)
    slot_ids = jnp.sum(before * onehot.astype(jnp.float32), axis=1).astype(jnp.int32)
    return (flat_ids * capacity + slot_ids).reshape(tokens, choices)


def body(
    stream,
    queries,
    key_rows,
    values,
    out_gate,
    fwd_decay,
    bwd_decay,
    head_gain,
    out_proj,
    mix_gain,
    ffn_gain,
    moe_gain,
    routes,
    route_weight,
    expert_gate,
    expert_up,
    expert_down,
    shared_gate,
    shared_up,
    shared_down,
):
    tokens_here = stream.shape[0]
    span_rows = queries.shape[0]
    experts = lax.axis_size("sp")
    capacity = max(2, 3 * tokens_here * TOPK // (2 * experts))
    gate_parts = lax.all_gather(expert_gate[0], "tp")
    up_parts = lax.all_gather(expert_up[0], "tp")
    down_mat = lax.all_gather(expert_down[0], "tp", axis=0, tiled=True)
    rows_of = slot_map(routes, experts, capacity)
    slots = jnp.arange(experts * capacity, dtype=jnp.int32)
    taken = rows_of[:, :, None] == slots[None, None, :]
    pick = jnp.any(taken, axis=1).astype(jnp.bfloat16)
    weights = jnp.sum(jnp.where(taken, route_weight[:, :, None], 0.0), axis=1)
    weights = weights.reshape(tokens_here, experts, capacity).transpose(1, 0, 2)
    weights_high = weights.astype(jnp.bfloat16)
    weights_low = (weights - weights_high.astype(jnp.float32)).astype(jnp.bfloat16)
    offset = lax.axis_index("sp") * span_rows
    positions = (offset + jnp.arange(span_rows, dtype=jnp.int32)).astype(jnp.float32)
    lanes = queries.shape[1]
    half = KEY_CHANNELS // 2
    lane = jnp.arange(lanes, dtype=jnp.int32) % KEY_CHANNELS
    frequency = ROPE_BASE ** (-(lane % half).astype(jnp.float32) / half)
    angles = positions[:, None] * frequency[None, :]
    sine = jnp.sin(angles)
    mixed_out = attention(
        queries,
        key_rows,
        values,
        out_gate,
        jax.nn.log_sigmoid(fwd_decay) / GATE_NORM,
        jax.nn.log_sigmoid(bwd_decay) / GATE_NORM,
        jnp.cos(angles),
        jnp.where(lane[None, :] < half, -sine, sine),
        head_gain.reshape(1, -1),
    )
    projected = jnp.dot(mixed_out, out_proj, preferred_element_type=jnp.float32)
    residual = (stream.astype(jnp.float32) + normalize(projected) * mix_gain).astype(jnp.bfloat16)
    normed = (normalize(residual.astype(jnp.float32)) * ffn_gain).astype(jnp.bfloat16)
    model_width = normed.shape[1]
    outgoing = lax.dot_general(
        pick, normed, (((0,), (0,)), ((), ())), preferred_element_type=jnp.float32
    ).astype(jnp.bfloat16)
    arrived, shared_sum, parts = dispatch(
        outgoing.reshape(experts, capacity, model_width),
        normed,
        shared_gate,
        shared_up,
        shared_down,
    )
    return run_expert(
        arrived.reshape(experts * capacity, model_width),
        gate_parts,
        up_parts,
        down_mat,
        weights_high,
        weights_low,
        shared_sum,
        parts,
        residual,
        moe_gain.reshape(1, -1),
    )


def solution(mesh):
    return jax.shard_map(
        body,
        mesh=mesh,
        in_specs=(
            P(("sp", "tp"), None),
            P("sp", "tp"),
            P("sp", "tp"),
            P("sp", "tp"),
            P("sp", "tp"),
            P("sp", "tp"),
            P("sp", "tp"),
            P("tp"),
            P(),
            P(),
            P(),
            P(),
            P(("sp", "tp"), None),
            P(("sp", "tp"), None),
            P("sp", None, "tp"),
            P("sp", None, "tp"),
            P("sp", "tp", None),
            P(None, "tp"),
            P(None, "tp"),
            P("tp", None),
        ),
        out_specs=P(("sp", "tp"), None),
        check_vma=False,
    )
```

profile of v0, /device:TPU:10, one launch (start us, length us, event | category | flops | bytes accessed | tf_op | source)
XLA Modules:
  0.0 195.3 jit_solution(17968594633149369453)
XLA Ops:
  6.5 0.0 all-gather.5.cloned.1.call-start
  6.5 0.7 all-gather.5.cloned.1.call-update
  7.3 0.0 all-gather.7.cloned.1.call-start
  7.3 0.7 all-gather.7.cloned.1.call-update
  8.0 0.0 all-gather.9.cloned.1.call-start
  8.1 0.7 all-gather.9.cloned.1.call-update
  8.7 0.8 copy.39
  9.5 0.1 eq.31
  9.7 0.2 fusion
  9.9 0.1 convert_element_type.57
  10.0 0.1 copy.40
  10.1 0.7 multiply_add_fusion
  10.8 0.8 select_reduce_fusion
  11.6 0.1 copy.41
  11.8 0.2 copy.42
  12.0 1.9 negate_select_fusion
  13.9 0.0 copy-start.5
  13.9 1.1 fusion.7
  15.0 25.9 %shard_map.190 = bf16[128,1024]{1,0:T(8,128)(2,1)} custom-call(bf16[512,128]{1,0:T(8,128)(2,1)} %q_ref.1, bf16[512,128]{1,0:T(8,128)(2,1)} %k_ref.1, bf16[512,256]{1,0:T(8,128)(2,1)} %v_ref.1, bf16[512,256]{1,0:T(8,128)(2,1)} %gate_ref.2, f32[512,128]{1,0:T(8,128)} %get-tuple-element.19.fwd_ref, f32[512,128]{1,0:T(8,128)} %get-tuple-element.20.bwd_ref, ...), custom_call_target="tpu_custom_call" | custom-call | tf_op jit(solution)/shard_map/pallas_call | solution.py:259
  40.9 0.0 copy-start.6
  40.9 0.1 fusion.5
  41.1 3.1 %multiply_reduce_fusion = (f32[128]{0:T(128)S(1)}, f32[128,2048]{1,0:T(8,128)S(1)}) fusion(bf16[128,1024]{1,0:T(8,128)(2,1)} %shard_map.190, bf16[1024,2048]{1,0:T(8,128)(2,1)} %param.28), kind=kOutput, calls=%fused_computation.9 | convolution fusion | flops 537395072 | bytes 5505536 | tf_op jit(solution)/shard_map/dot_general | solution.py:613
  44.2 0.4 fusion.1
  44.6 0.2 fusion.3.rows_ref
  44.8 0.0 copy-start.1
  44.8 1.8 convolution_convert_fusion
  46.5 45.7 %shard_map.191 = (bf16[8,48,2048]{2,1,0:T(8,128)(2,1)}, f32[128,2048]{1,0:T(8,128)}, bf16[4,128,2048]{2,1,0:T(8,128)(2,1)}) custom-call(bf16[8,48,2048]{2,1,0:T(8,128)(2,1)} %bitcast.16, bf16[128,2048]{1,0:T(8,128)(2,1)} %copy-done.1, bf16[2048,128]{1,0:T(8,128)(2,1)} %gate_ref.3, bf16[2048,128]{1,0:T(8,128)(2,1)} %up_ref.1, bf16[128,2048]{1,0:T(8,128)(2,1)} %down_ref.1), custom_call_target="tpu_custom_call" | custom-call | tf_op jit(solution)/shard_map/pallas_call | solution.py:364
  92.2 0.9 fusion.4
  93.1 7.3 %all-gather.7.cloned.1.call-done.up_hbm = bf16[4,2048,256]{2,1,0:T(8,128)(2,1)} async-done(((bf16[1,2048,256]{2,1,0:T(8,128)(2,1)}), bf16[4,2048,256]{2,1,0:T(8,128)(2,1)}) %all-gather.7.cloned.1.call-update) | async-done | bytes 4194320 | tf_op jit(solution)/shard_map/all_gather | solution.py:584
  100.5 35.4 %all-gather.9.cloned.1.call-done = bf16[1,1024,2048]{2,1,0:T(8,128)(2,1)} async-done(((bf16[1,256,2048]{2,1,0:T(8,128)(2,1)}), bf16[1,1024,2048]{2,1,0:T(8,128)(2,1)}) %all-gather.9.cloned.1.call-update) | async-done | bytes 4194320 | tf_op jit(solution)/shard_map/all_gather | solution.py:585
  135.9 51.0 %shard_map.192 = bf16[128,2048]{1,0:T(8,128)(2,1)} custom-call(bf16[384,2048]{1,0:T(8,128)(2,1)} %bitcast.18, bf16[4,2048,256]{2,1,0:T(8,128)(2,1)} %all-gather.5.cloned.1.call-done.gate_hbm, bf16[4,2048,256]{2,1,0:T(8,128)(2,1)} %all-gather.7.cloned.1.call-done.up_hbm, bf16[1024,2048]{1,0:T(8,128)(2,1)} %bitcast.17, ...), custom_call_target="tpu_custom_call" | custom-call | tf_op jit(solution)/shard_map/pallas_call | solution.py:521
  186.9 1.9 copy.44
  (18 shorter events, 0.1 us)
Async XLA Ops:
  6.5 7.3 %copy-start.3 = (f32[512,128]{1,0:T(8,128)S(1)}, f32[512,128]{1,0:T(8,128)}, u32[]{:S(2)}) copy-start(f32[512,128]{1,0:T(8,128)} %param.25) | copy-start | bytes 786436
  6.5 7.3 %copy-start.4 = (f32[512,128]{1,0:T(8,128)S(1)}, f32[512,128]{1,0:T(8,128)}, u32[]{:S(2)}) copy-start(f32[512,128]{1,0:T(8,128)} %param.26) | copy-start | bytes 786436
  6.5 86.6 %all-gather.5.cloned.1.call-start = ((), (), s32[]{:S(2)}) async-start(), calls=%async_computation | async-start | bytes 5242880 | tf_op jit(solution)/shard_map/all_gather | solution.py:583
  7.3 93.2 %all-gather.7.cloned.1.call-start = ((), (), s32[]{:S(2)}) async-start(), calls=%async_computation.1 | async-start | bytes 5242880 | tf_op jit(solution)/shard_map/all_gather | solution.py:584
  8.0 127.9 %all-gather.9.cloned.1.call-start = ((), (), s32[]{:S(2)}) async-start(), calls=%async_computation.2 | async-start | bytes 5242880 | tf_op jit(solution)/shard_map/all_gather | solution.py:585
  13.9 30.3 %copy-start.2 = (bf16[128,2048]{1,0:T(8,128)(2,1)S(1)}, bf16[128,2048]{1,0:T(8,128)(2,1)}, u32[]{:S(2)}) copy-start(bf16[128,2048]{1,0:T(8,128)(2,1)} %param.20) | copy-start | bytes 1572868
  13.9 30.3 %copy-start.5 = (f32[2048]{0:T(1024)S(1)}, f32[2048]{0:T(1024)}, u32[]{:S(2)}) copy-start(f32[2048]{0:T(1024)} %param.29) | copy-start | bytes 24580
  40.9 3.6 %copy-start.6 = (f32[2048]{0:T(1024)S(1)}, f32[2048]{0:T(1024)}, u32[]{:S(2)}) copy-start(f32[2048]{0:T(1024)} %param.30) | copy-start | bytes 24580
  44.6 91.3 %copy-start = (bf16[128,2048]{1,0:T(8,128)(2,1)}, bf16[128,2048]{1,0:T(8,128)(2,1)S(1)}, u32[]{:S(2)}) copy-start(bf16[128,2048]{1,0:T(8,128)(2,1)S(1)} %get-tuple-element.14.residual_ref) | copy-start | bytes 1572868
  44.8 1.8 copy-start.1
Sparse Core Ops, SparseCore 0:
  8.9 38.3 all-gather.4
  48.9 51.5 all-gather.6
  102.0 33.8 all-gather.8
where the time goes:
time: 196 us; the launch traced here: 195 us
  Pallas kernels  123 us (63%)
  waiting for transfers between devices  44.9 us (23%)
  between operations  13.3 us (7%)
  other arithmetic  6.11 us (3%)
  matrix products  5.04 us (3%)
  local copies, waits for them, and re-layouts  3.35 us (2%)
    pallas_call x1, Pallas kernels, run_expert(): pl.pallas_call(functools.partial(expert_kernel, sp_count, lax.axis_size('...  51 us
    pallas_call x1, Pallas kernels, dispatch(): pl.pallas_call(functools.partial(dispatch_kernel, sp_count, tp_count), ou...  45.7 us
    all_gather x1, waiting for transfers between devices, body(): down_mat = lax.all_gather(expert_down[0], 'tp', axis=0, tiled=True)  35.4 us
    pallas_call x1, Pallas kernels, attention(): pl.pallas_call(functools.partial(attention_kernel, sp_count, tp_count), o...  25.9 us
    all_gather x1, waiting for transfers between devices, body(): up_parts = lax.all_gather(expert_up[0], 'tp')  7.34 us
  transfers between devices with their start and end apart: 3, of which 2 were waited for; matrix products, arithmetic and copies ran while one was open for 6% of the time, Pallas kernels for 37%

commit v1 on v0

v1 whole, which is shorter than its diff:
```python
import functools

import jax
import jax.numpy as jnp
from jax import lax
from jax.experimental import pallas as pl
from jax.experimental.pallas import tpu as pltpu
from jax.sharding import PartitionSpec as P

KEY_CHANNELS = 64
DV = 128
BLK = 64
TOPK = 2
ROW_TILE = 16


EPS = 1e-06
GATE_NORM = 16.0
ROPE_BASE = 10000.0
MESH = pl.DeviceIdType.MESH
WEIGHT_CUTS = 4
WEIGHT_EARLY = 4


def dot_nn(left, right):
    return jnp.dot(left, right, preferred_element_type=jnp.float32)


def dot_nt(left, right):
    return lax.dot_general(
        left, right, (((1,), (1,)), ((), ())), preferred_element_type=jnp.float32
    )


def dot_tn(left, right):
    return lax.dot_general(
        left, right, (((0,), (0,)), ((), ())), preferred_element_type=jnp.float32
    )


def layer_kernel(
    sp_count,
    tp_count,
    capacity,
    return_cuts,
    q_ref,
    k_ref,
    v_ref,
    fwd_ref,
    bwd_ref,
    table_ref,
    gain_ref,
    mix_gain_ref,
    ffn_gain_ref,
    moe_gain_ref,
    routes_ref,
    route_weight_ref,
    out_gate_hbm,
    stream_hbm,
    proj_hbm,
    gate_hbm,
    up_hbm,
    down_hbm,
    shared_gate_hbm,
    shared_up_hbm,
    shared_down_hbm,
    out_ref,
    out_gate_ref,
    stream_ref,
    proj_ref,
    gate_ref,
    up_ref,
    down_ref,
    sgate_ref,
    sup_ref,
    sdown_ref,
    own_ref,
    got_ref,
    mixed_ref,
    land_ref,
    within_ref,
    key_ref,
    sums_f,
    sums_b,
    heads_ref,
    wide_ref,
    residual_ref,
    normed_ref,
    outgoing_ref,
    arrived_ref,
    hidden_ref,
    done_ref,
    back_ref,
    local_sem,
    sum_send,
    sum_recv,
    row_send,
    row_recv,
    block_send,
    block_recv,
    back_send,
    back_recv,
    weight_sem,
    pair_send,
    pair_recv,
    cross_send,
    cross_recv,
    relay_send,
    relay_recv,
    near_send,
    near_recv,
    slice_send,
    slice_recv,
    spread_send,
    spread_recv,
    side_send,
    side_recv,
    last_send,
    last_recv,
):
    span, lanes = q_ref.shape
    width = v_ref.shape[1]
    heads = lanes // KEY_CHANNELS
    blocks = span // BLK
    tokens = span // tp_count
    model = stream_ref.shape[1]
    part_width = gate_ref.shape[2]
    slots = sp_count * capacity
    cut = model // return_cuts
    piece = model // WEIGHT_CUTS
    sp_me = lax.axis_index("sp")
    tp_me = lax.axis_index("tp")
    ranks = tp_count // 2
    rank = lax.div(tp_me, 2)
    seat = lax.rem(tp_me, 2)
    buddy = (sp_me, tp_me + 1 - 2 * seat)
    team = min(8, sp_count)
    place = lax.rem(sp_me, team)
    team_base = sp_me - place
    sends = []

    def sp_peer(step):
        return (lax.rem(sp_me + step, sp_count), tp_me)

    def tp_peer(step):
        return (sp_me, lax.rem(tp_me + step, tp_count))

    def cross_tp(step):
        return lax.rem(rank + step, ranks) * 2 + seat

    def send(source, target, send_sem, recv_sem, device):
        copy = pltpu.make_async_remote_copy(
            src_ref=source,
            dst_ref=target,
            send_sem=send_sem,
            recv_sem=recv_sem,
            device_id=device,
            device_id_type=MESH,
        )
        copy.start()
        sends.append(copy)
        return copy

    def fetch(source, target, semaphore):
        copy = pltpu.make_async_copy(source, target, semaphore)
        copy.start()
        return copy

    barrier = pltpu.get_barrier_semaphore()
    for step in range(1, sp_count):
        pl.semaphore_signal(barrier, inc=1, device_id=sp_peer(step), device_id_type=MESH)
    for step in range(1, tp_count):
        pl.semaphore_signal(barrier, inc=1, device_id=tp_peer(step), device_id_type=MESH)

    def weight_source(index):
        kind, at = divmod(index, WEIGHT_CUTS)
        if kind < 2:
            return (gate_hbm, up_hbm)[kind].at[0, pl.ds(at * piece, piece), :]
        return down_hbm.at[0, :, pl.ds(at * piece, piece)]

    def weight_slot(index, owner):
        kind, at = divmod(index, WEIGHT_CUTS)
        if kind < 2:
            return (gate_ref, up_ref)[kind].at[owner, pl.ds(at * piece, piece), :]
        row = pl.multiple_of(owner * part_width, part_width)
        return down_ref.at[at, pl.ds(row, part_width), :]

    shared_lanes = shared_gate_hbm.shape[1]

    def shared_slot(kind, owner, which=None):
        column = pl.ds(pl.multiple_of(owner * shared_lanes, shared_lanes), shared_lanes)
        if kind < 2:
            ref = (sgate_ref, sup_ref)[kind]
            if which is None:
                return ref.at[:, column]
            size = model // team
            return ref.at[pl.ds(pl.multiple_of(which * size, size), size), column]
        if which is None:
            return sdown_ref.at[column, :]
        size = shared_lanes // team
        row = pl.multiple_of(owner * shared_lanes + which * size, size)
        return sdown_ref.at[pl.ds(row, size), :]

    def shared_source(kind, which=None):
        ref = (shared_gate_hbm, shared_up_hbm, shared_down_hbm)[kind]
        if which is None:
            return ref
        size = (shared_lanes if kind == 2 else model) // team
        return ref.at[pl.ds(pl.multiple_of(which * size, size), size), :]

    count = 3 * WEIGHT_CUTS
    gate_fetch = fetch(out_gate_hbm, out_gate_ref, local_sem.at[0])
    stream_fetch = fetch(stream_hbm, stream_ref, local_sem.at[1])
    proj_fetch = fetch(proj_hbm, proj_ref, local_sem.at[2])
    shared_fetches = [
        fetch(shared_source(kind), shared_slot(kind, tp_me), local_sem.at[3 + kind])
        for kind in range(3)
    ]
    weight_fetches = [
        fetch(weight_source(index), weight_slot(index, tp_me), weight_sem.at[index])
        for index in range(count)
    ]

    row = lax.broadcasted_iota(jnp.int32, (BLK, BLK), 0)
    column = lax.broadcasted_iota(jnp.int32, (BLK, BLK), 1)
    lower = row >= column
    upper = row <= column
    lower_ones = lower.astype(jnp.bfloat16)
    upper_ones = upper.astype(jnp.bfloat16)
    from_lane = lax.broadcasted_iota(jnp.int32, (lanes, lanes), 0)
    to_lane = lax.broadcasted_iota(jnp.int32, (lanes, lanes), 1)
    half = KEY_CHANNELS // 2
    partner = jnp.where(lax.rem(to_lane, KEY_CHANNELS) < half, to_lane + half, to_lane - half)
    swap = (from_lane == partner).astype(jnp.bfloat16)
    own_head = (
        lax.broadcasted_iota(jnp.int32, (width, lanes), 0) // DV
        == lax.broadcasted_iota(jnp.int32, (width, lanes), 1) // KEY_CHANNELS
    )
    lane_head = lax.broadcasted_iota(jnp.int32, (BLK, lanes), 1) // KEY_CHANNELS

    cos_row, sin_row = table_ref[0, 0:BLK, :], table_ref[1, 0:BLK, :]

    def rotated(tensor, block):
        cos_at = table_ref[0, BLK + block : BLK + block + 1, :]
        sin_at = table_ref[1, BLK + block : BLK + block + 1, :]
        cosine = cos_row * cos_at - sin_row * sin_at
        sine = sin_row * cos_at + cos_row * sin_at
        return tensor.astype(jnp.float32) * cosine + dot_nn(tensor, swap) * sine

    def running(ones, raw):
        logs = (jnp.minimum(raw, 0.0) - jnp.log1p(jnp.exp(-jnp.abs(raw)))) * (1.0 / GATE_NORM)
        first = logs.astype(jnp.bfloat16)
        rest = logs - first.astype(jnp.float32)
        second = rest.astype(jnp.bfloat16)
        third = (rest - second.astype(jnp.float32)).astype(jnp.bfloat16)
        return dot_nn(ones, first) + (dot_nn(ones, second) + dot_nn(ones, third))

    pl.semaphore_wait(barrier, sp_count - 1 + tp_count - 1)

    near, slices = [], []
    for kind in range(3):
        for step in range(1, ranks):
            slices.append(
                send(
                    shared_source(kind, place),
                    shared_slot(kind, tp_me, place),
                    slice_send.at[step, kind],
                    slice_recv.at[step, kind],
                    (sp_me, cross_tp(step)),
                )
            )

    crossings = {}

    def cross(index):
        crossings[index] = [
            send(
                weight_source(index),
                weight_slot(index, tp_me),
                cross_send.at[step, index],
                cross_recv.at[step, index],
                (sp_me, cross_tp(step)),
            )
            for step in range(1, ranks)
        ]

    relays = {}

    def relay(index):
        relays[index] = []
        for step in range(1, ranks):
            crossings[index][step - 1].wait_recv()
            owner = lax.rem(rank + ranks - step, ranks) * 2 + seat
            relays[index].append(
                send(
                    weight_slot(index, owner),
                    weight_slot(index, owner),
                    relay_send.at[step, index],
                    relay_recv.at[step, index],
                    buddy,
                )
            )

    cross(0)
    cross(1)
    for kind in range(3):
        near.append(
            send(
                shared_source(kind),
                shared_slot(kind, tp_me),
                near_send.at[kind],
                near_recv.at[kind],
                buddy,
            )
        )
    pairs = [
        send(
            weight_source(index),
            weight_slot(index, tp_me),
            pair_send.at[index],
            pair_recv.at[index],
            buddy,
        )
        for index in range(count)
    ]

    cumul_f, cumul_b, decay_f, decay_b = [], [], [], []
    for block in range(blocks):
        rows = pl.ds(block * BLK, BLK)
        total_f = running(lower_ones, fwd_ref[rows, :])
        total_b = running(upper_ones, bwd_ref[rows, :])
        last_f = total_f[BLK - 1 : BLK]
        last_b = total_b[0:1]
        keys = rotated(k_ref[rows, :], block)
        key_ref[rows, :] = keys
        value_rows = v_ref[rows, :]
        out_f = (keys * jnp.exp(last_f - total_f)).astype(jnp.bfloat16)
        out_b = (keys * jnp.exp(last_b - total_b)).astype(jnp.bfloat16)
        sums_f[block] = jnp.where(own_head, dot_tn(value_rows, out_f), 0.0)
        sums_b[block] = jnp.where(own_head, dot_tn(value_rows, out_b), 0.0)
        cumul_f.append(total_f)
        cumul_b.append(total_b)
        decay_f.append(jnp.exp(last_f))
        decay_b.append(jnp.exp(last_b))

    def packed(total):
        return sum(total[h * DV : (h + 1) * DV] for h in range(heads))

    total = sums_f[0]
    through = decay_f[0]
    for block in range(1, blocks):
        total = total * decay_f[block] + sums_f[block]
        through = through * decay_f[block]
    own_ref[0, 0:DV, :] = packed(total).astype(jnp.bfloat16)
    own_ref[0, DV : DV + 16, :] = jnp.broadcast_to(through, (16, lanes)).astype(jnp.bfloat16)
    total = sums_b[blocks - 1]
    through = decay_b[blocks - 1]
    for block in range(blocks - 2, -1, -1):
        total = total * decay_b[block] + sums_b[block]
        through = through * decay_b[block]
    own_ref[1, 0:DV, :] = packed(total).astype(jnp.bfloat16)
    own_ref[1, DV : DV + 16, :] = jnp.broadcast_to(through, (16, lanes)).astype(jnp.bfloat16)

    sum_copies = [
        send(
            own_ref.at[lax.div(sp_me + step, sp_count)],
            got_ref.at[step],
            sum_send.at[step],
            sum_recv.at[step],
            sp_peer(step),
        )
        for step in range(1, sp_count)
    ]
    cross(2)

    spreads = []
    for copy in slices:
        copy.wait_recv()
    for hop in range(1, team // 2):
        to_place = lax.rem(place + 2 * hop, team)
        for step in range(1, ranks):
            owner = lax.rem(rank + ranks - step, ranks) * 2 + seat
            for kind in range(3):
                spreads.append(
                    send(
                        shared_slot(kind, owner, place),
                        shared_slot(kind, owner, place),
                        spread_send.at[hop, step, kind],
                        spread_recv.at[hop, step, kind],
                        (team_base + to_place, tp_me),
                    )
                )

    query_f, query_b = [], []
    for block in range(blocks):
        rows = pl.ds(block * BLK, BLK)
        queries = rotated(q_ref[rows, :], block) * KEY_CHANNELS ** (-0.5)
        keys = key_ref[rows, :]
        total_f, total_b = cumul_f[block], cumul_b[block]
        middle_f = total_f[BLK // 2 - 1 : BLK // 2]
        middle_b = total_b[BLK // 2 : BLK // 2 + 1]
        scaled_qf = queries * jnp.exp(total_f - middle_f)
        scaled_qb = queries * jnp.exp(total_b - middle_b)
        scaled_kf = (keys * jnp.exp(middle_f - total_f)).astype(jnp.bfloat16)
        scaled_kb = (keys * jnp.exp(middle_b - total_b)).astype(jnp.bfloat16)
        query_f.append((queries * jnp.exp(total_f)).astype(jnp.bfloat16))
        query_b.append((queries * jnp.exp(total_b)).astype(jnp.bfloat16))
        for h in range(heads):
            mine = lane_head == h
            scores_f = dot_nt(jnp.where(mine, scaled_qf, 0.0).astype(jnp.bfloat16), scaled_kf)
            scores_b = dot_nt(jnp.where(mine, scaled_qb, 0.0).astype(jnp.bfloat16), scaled_kb)
            scores = jnp.where(lower, scores_f, 0.0) + jnp.where(upper, scores_b, 0.0)
            within_ref[rows, h * DV : (h + 1) * DV] = dot_nn(
                scores.astype(jnp.bfloat16), v_ref[rows, h * DV : (h + 1) * DV]
            )
    for index in range(3, WEIGHT_EARLY):
        cross(index)

    for copy in sum_copies:
        copy.wait_recv()
    carry_f = jnp.zeros((DV, lanes), jnp.float32)
    carry_b = jnp.zeros((DV, lanes), jnp.float32)
    for step in range(sp_count - 1, 0, -1):
        state = got_ref[step, 0:DV, :].astype(jnp.float32)
        through = got_ref[step, DV : DV + 16, :].astype(jnp.float32)[0:1]
        carry_f = jnp.where(step <= sp_me, carry_f * through + state, carry_f)
    for step in range(1, sp_count):
        state = got_ref[step, 0:DV, :].astype(jnp.float32)
        through = got_ref[step, DV : DV + 16, :].astype(jnp.float32)[0:1]
        carry_b = jnp.where(step > sp_me, carry_b * through + state, carry_b)

    def unpacked(carry):
        return jnp.where(own_head, jnp.concatenate([carry] * heads, axis=0), 0.0)

    state = unpacked(carry_f)
    for block in range(blocks):
        rows = pl.ds(block * BLK, BLK)
        within_ref[rows, :] += dot_nt(query_f[block], state.astype(jnp.bfloat16))
        if block < blocks - 1:
            state = state * decay_f[block] + sums_f[block]
    gate_fetch.wait()
    state = unpacked(carry_b)
    for block in range(blocks - 1, -1, -1):
        rows = pl.ds(block * BLK, BLK)
        attended = within_ref[rows, :] + dot_nt(query_b[block], state.astype(jnp.bfloat16))
        if block > 0:
            state = state * decay_b[block] + sums_b[block]
        for h in range(heads):
            part = attended[:, h * DV : (h + 1) * DV]
            square = jnp.mean(part * part, axis=-1, keepdims=True)
            gate = out_gate_ref[rows, h * DV : (h + 1) * DV].astype(jnp.float32)
            mixed_ref[rows, h * DV : (h + 1) * DV] = (
                part
                * lax.rsqrt(square + EPS)
                * gain_ref[:, h * DV : (h + 1) * DV]
                * (gate / (1.0 + jnp.exp(-gate)))
            ).astype(jnp.bfloat16)

    row_copies = []
    for step in range(1, tp_count):
        target = lax.rem(tp_me + step, tp_count)
        row_copies.append(
            send(
                mixed_ref.at[pl.ds(pl.multiple_of(target * tokens, tokens), tokens)],
                land_ref.at[tp_me],
                row_send.at[step],
                row_recv.at[step],
                (sp_me, target),
            )
        )
    for index in range(WEIGHT_EARLY, count):
        cross(index)
    land_ref[tp_me] = mixed_ref[pl.ds(pl.multiple_of(tp_me * tokens, tokens), tokens), :]

    token_row = lax.broadcasted_iota(jnp.int32, (tokens, tokens), 0)
    token_column = lax.broadcasted_iota(jnp.int32, (tokens, tokens), 1)
    earlier = (token_row > token_column).astype(jnp.bfloat16)
    expert_lane = lax.broadcasted_iota(jnp.int32, (tokens, 128), 1)
    choices = [routes_ref[:, choice : choice + 1] for choice in range(TOPK)]
    named = [(chosen == expert_lane).astype(jnp.float32) for chosen in choices]
    before = dot_nn(earlier, sum(named).astype(jnp.bfloat16))
    slot_lane = lax.broadcasted_iota(jnp.int32, (tokens, slots), 1).astype(jnp.float32)
    weights = jnp.zeros((tokens, slots), jnp.float32)
    picked = jnp.zeros((tokens, slots), jnp.float32)
    for choice in range(TOPK):
        slot = jnp.sum(before * named[choice], axis=1, keepdims=True)
        place_of = choices[choice].astype(jnp.float32) * capacity + slot
        hit = slot_lane == place_of
        picked = jnp.where(hit, 1.0, picked)
        weights = jnp.where(hit, route_weight_ref[:, choice : choice + 1], weights)
    picked = picked.astype(jnp.bfloat16)
    weights_high = weights.astype(jnp.bfloat16)
    weights_low = (weights - weights_high.astype(jnp.float32)).astype(jnp.bfloat16)

    for copy in row_copies:
        copy.wait_recv()
    for source in range(tp_count):
        heads_ref[:, source * width : (source + 1) * width] = land_ref[source]
    proj_fetch.wait()
    stream_fetch.wait()
    square = jnp.zeros((tokens, 1), jnp.float32)
    for at in range(0, model, 512):
        part = dot_nn(heads_ref[...], proj_ref[:, at : at + 512])
        wide_ref[:, at : at + 512] = part
        square = square + jnp.sum(part * part, axis=-1, keepdims=True)
    scale = lax.rsqrt(square * (1.0 / model) + EPS)
    square = jnp.zeros((tokens, 1), jnp.float32)
    for at in range(0, model, 512):
        part = (
            stream_ref[:, at : at + 512].astype(jnp.float32)
            + wide_ref[:, at : at + 512] * scale * mix_gain_ref[:, at : at + 512]
        ).astype(jnp.bfloat16)
        residual_ref[:, at : at + 512] = part
        part = part.astype(jnp.float32)
        square = square + jnp.sum(part * part, axis=-1, keepdims=True)
    scale = lax.rsqrt(square * (1.0 / model) + EPS)
    for at in range(0, model, 512):
        part = (
            residual_ref[:, at : at + 512].astype(jnp.float32)
            * scale
            * ffn_gain_ref[:, at : at + 512]
        ).astype(jnp.bfloat16)
        normed_ref[:, at : at + 512] = part
        outgoing_ref[:, :, at : at + 512] = (
            dot_tn(picked, part).astype(jnp.bfloat16).reshape(sp_count, capacity, 512)
        )

    block_copies = [
        send(
            outgoing_ref.at[lax.rem(sp_me + step, sp_count)],
            arrived_ref.at[sp_me],
            block_send.at[step],
            block_recv.at[step],
            sp_peer(step),
        )
        for step in range(1, sp_count)
    ]
    arrived_ref[sp_me] = outgoing_ref[sp_me]

    for index in range(WEIGHT_EARLY):
        relay(index)
    for copy in spreads:
        copy.wait_recv()
    sides = []
    side = sp_me + 1 - 2 * lax.rem(sp_me, 2)
    for hop in range(team // 2):
        which = lax.rem(place + 2 * hop, team)
        for step in range(1, ranks):
            owner = lax.rem(rank + ranks - step, ranks) * 2 + seat
            for kind in range(3):
                sides.append(
                    send(
                        shared_slot(kind, owner, which),
                        shared_slot(kind, owner, which),
                        side_send.at[hop, step, kind],
                        side_recv.at[hop, step, kind],
                        (side, tp_me),
                    )
                )
    relay(WEIGHT_EARLY)
    relay(WEIGHT_EARLY + 1)
    for copy in sides:
        copy.wait_recv()
    lasts = []
    for step in range(1, ranks):
        owner = lax.rem(rank + ranks - step, ranks) * 2 + seat
        for kind in range(3):
            lasts.append(
                send(
                    shared_slot(kind, owner),
                    shared_slot(kind, owner),
                    last_send.at[step, kind],
                    last_recv.at[step, kind],
                    buddy,
                )
            )
    relay(WEIGHT_EARLY + 2)
    for copy in shared_fetches:
        copy.wait()
    for copy in near + lasts:
        copy.wait_recv()
    shared_hidden = jax.nn.silu(dot_nn(normed_ref[...], sgate_ref[...])) * dot_nn(
        normed_ref[...], sup_ref[...]
    )
    shared_hidden = shared_hidden.astype(jnp.bfloat16)
    for at in range(0, model, 512):
        wide_ref[:, at : at + 512] = dot_nn(shared_hidden, sdown_ref[:, at : at + 512])

    relay(WEIGHT_EARLY + 3)
    for index in range(2 * WEIGHT_CUTS):
        weight_fetches[index].wait()
        pairs[index].wait_recv()
        for copy in relays[index]:
            copy.wait_recv()
    relay(2 * WEIGHT_CUTS)
    for copy in block_copies:
        copy.wait_recv()
    rows_in = arrived_ref[...].reshape(slots, model)
    for owner in range(tp_count):
        hidden_ref[:, owner * part_width : (owner + 1) * part_width] = (
            jax.nn.silu(dot_nn(rows_in, gate_ref[owner])) * dot_nn(rows_in, up_ref[owner])
        ).astype(jnp.bfloat16)

    returns = []
    per_cut = WEIGHT_CUTS // return_cuts
    for part in range(return_cuts):
        for at in range(part * per_cut, (part + 1) * per_cut):
            index = 2 * WEIGHT_CUTS + at
            if at > 0:
                relay(index)
            weight_fetches[index].wait()
            pairs[index].wait_recv()
            for copy in relays[index]:
                copy.wait_recv()
            inner = pl.ds((at - part * per_cut) * piece, piece)
            done_ref[part, :, :, inner] = (
                dot_nn(hidden_ref[...], down_ref[at])
                .astype(jnp.bfloat16)
                .reshape(sp_count, capacity, piece)
            )
        returns.append(
            [
                send(
                    done_ref.at[part, lax.rem(sp_me + step, sp_count)],
                    back_ref.at[part, sp_me],
                    back_send.at[part, step],
                    back_recv.at[part, step],
                    sp_peer(step),
                )
                for step in range(1, sp_count)
            ]
        )
        back_ref[part, sp_me] = done_ref[part, sp_me]

    square = jnp.zeros((tokens, 1), jnp.float32)
    for part in range(return_cuts):
        for copy in returns[part]:
            copy.wait_recv()
        back = back_ref[part].reshape(slots, cut)
        inner = pl.ds(part * cut, cut)
        mixture = wide_ref[:, inner] + dot_nn(weights_high, back) + dot_nn(weights_low, back)
        wide_ref[:, inner] = mixture
        square = square + jnp.sum(mixture * mixture, axis=-1, keepdims=True)
    scale = lax.rsqrt(square * (1.0 / model) + EPS)
    for at in range(0, model, 512):
        out_ref[:, at : at + 512] = (
            residual_ref[:, at : at + 512].astype(jnp.float32)
            + wide_ref[:, at : at + 512] * scale * moe_gain_ref[:, at : at + 512]
        ).astype(out_ref.dtype)
    for copy in sends:
        copy.wait_send()


def body(
    stream,
    queries,
    key_rows,
    values,
    out_gate,
    fwd_decay,
    bwd_decay,
    head_gain,
    out_proj,
    mix_gain,
    ffn_gain,
    moe_gain,
    routes,
    route_weight,
    expert_gate,
    expert_up,
    expert_down,
    shared_gate,
    shared_up,
    shared_down,
):
    sp_count = lax.axis_size("sp")
    tp_count = lax.axis_size("tp")
    tokens, model = stream.shape
    span, lanes = queries.shape
    width = values.shape[1]
    blocks = span // BLK
    part_width = expert_gate.shape[2]
    shared_width = shared_gate.shape[1] * tp_count
    capacity = max(2, 3 * tokens * TOPK // (2 * sp_count))
    capacity = -(-capacity // ROW_TILE) * ROW_TILE
    slots = sp_count * capacity
    return_cuts = WEIGHT_CUTS if sp_count <= 16 else 1
    team = min(8, sp_count)
    ranks = tp_count // 2

    half = KEY_CHANNELS // 2
    lane = jnp.arange(lanes, dtype=jnp.int32) % KEY_CHANNELS
    frequency = ROPE_BASE ** (-(lane % half).astype(jnp.float32) / half)
    offset = lax.axis_index("sp") * span
    index = jnp.arange(BLK + blocks, dtype=jnp.int32)
    positions = jnp.where(index < BLK, index, offset + (index - BLK) * BLK).astype(jnp.float32)
    angles = positions[:, None] * frequency[None, :]
    sine = jnp.sin(angles)
    table = jnp.stack([jnp.cos(angles), jnp.where(lane[None, :] < half, -sine, sine)])

    vmem = pl.BlockSpec(memory_space=pltpu.VMEM)
    hbm = pl.BlockSpec(memory_space=pl.ANY)
    dma = pltpu.SemaphoreType.DMA
    bf16, f32 = jnp.bfloat16, jnp.float32
    count = 3 * WEIGHT_CUTS
    return pl.pallas_call(
        functools.partial(layer_kernel, sp_count, tp_count, capacity, return_cuts),
        out_shape=jax.ShapeDtypeStruct(stream.shape, stream.dtype),
        in_specs=[vmem] * 12 + [hbm] * 9,
        out_specs=vmem,
        scratch_shapes=[
            pltpu.VMEM(out_gate.shape, bf16),
            pltpu.VMEM(stream.shape, bf16),
            pltpu.VMEM(out_proj.shape, bf16),
            pltpu.VMEM((tp_count, model, part_width), bf16),
            pltpu.VMEM((tp_count, model, part_width), bf16),
            pltpu.VMEM((WEIGHT_CUTS, tp_count * part_width, model // WEIGHT_CUTS), bf16),
            pltpu.VMEM((model, shared_width), bf16),
            pltpu.VMEM((model, shared_width), bf16),
            pltpu.VMEM((shared_width, model), bf16),
            pltpu.VMEM((2, DV + 16, lanes), bf16),
            pltpu.VMEM((sp_count, DV + 16, lanes), bf16),
            pltpu.VMEM((span, width), bf16),
            pltpu.VMEM((tp_count, tokens, width), bf16),
            pltpu.VMEM((span, width), f32),
            pltpu.VMEM((span, lanes), f32),
            pltpu.VMEM((blocks, width, lanes), f32),
            pltpu.VMEM((blocks, width, lanes), f32),
            pltpu.VMEM((tokens, tp_count * width), bf16),
            pltpu.VMEM((tokens, model), f32),
            pltpu.VMEM((tokens, model), bf16),
            pltpu.VMEM((tokens, model), bf16),
            pltpu.VMEM((sp_count, capacity, model), bf16),
            pltpu.VMEM((sp_count, capacity, model), bf16),
            pltpu.VMEM((slots, tp_count * part_width), bf16),
            pltpu.VMEM((return_cuts, sp_count, capacity, model // return_cuts), bf16),
            pltpu.VMEM((return_cuts, sp_count, capacity, model // return_cuts), bf16),
            dma((6,)),
            dma((sp_count,)),
            dma((sp_count,)),
            dma((tp_count,)),
            dma((tp_count,)),
            dma((sp_count,)),
            dma((sp_count,)),
            dma((return_cuts, sp_count)),
            dma((return_cuts, sp_count)),
            dma((count,)),
            dma((count,)),
            dma((count,)),
            dma((ranks, count)),
            dma((ranks, count)),
            dma((ranks, count)),
            dma((ranks, count)),
            dma((3,)),
            dma((3,)),
            dma((ranks, 3)),
            dma((ranks, 3)),
            dma((team // 2, ranks, 3)),
            dma((team // 2, ranks, 3)),
            dma((team // 2, ranks, 3)),
            dma((team // 2, ranks, 3)),
            dma((ranks, 3)),
            dma((ranks, 3)),
        ],
        compiler_params=pltpu.CompilerParams(
            collective_id=0, has_side_effects=True, vmem_limit_bytes=62 * 2**20
        ),
    )(
        queries,
        key_rows,
        values,
        fwd_decay,
        bwd_decay,
        table,
        head_gain.reshape(1, -1),
        mix_gain.reshape(1, -1),
        ffn_gain.reshape(1, -1),
        moe_gain.reshape(1, -1),
        routes,
        route_weight,
        out_gate,
        stream,
        out_proj,
        expert_gate,
        expert_up,
        expert_down,
        shared_gate,
        shared_up,
        shared_down,
    )


def solution(mesh):
    return jax.shard_map(
        body,
        mesh=mesh,
        in_specs=(
            P(("sp", "tp"), None),
            P("sp", "tp"),
            P("sp", "tp"),
            P("sp", "tp"),
            P("sp", "tp"),
            P("sp", "tp"),
            P("sp", "tp"),
            P("tp"),
            P(),
            P(),
            P(),
            P(),
            P(("sp", "tp"), None),
            P(("sp", "tp"), None),
            P("sp", None, "tp"),
            P("sp", None, "tp"),
            P("sp", "tp", None),
            P(None, "tp"),
            P(None, "tp"),
            P("tp", None),
        ),
        out_specs=P(("sp", "tp"), None),
        check_vma=False,
    )
```

time: 196 us -> 129 us (0.66)
  the two profiles are of different devices: /device:TPU:10 before, /device:TPU:0 now
where the time goes in v1:
time: 129 us; the launch traced here: 128 us
  Pallas kernels  123 us (95%)
  local copies, waits for them, and re-layouts  4.72 us (4%)
    pallas_call x1, Pallas kernels, body(): pl.pallas_call(functools.partial(layer_kernel, sp_count, tp_count, capaci...  123 us
    unnamed x3, local copies, waits for them, and re-layouts  4.72 us

profile of v1, /device:TPU:0, one launch (start us, length us, event | category | flops | bytes accessed | tf_op | source)
XLA Modules:
  0.0 128.2 jit_solution(4565157460547850928)
XLA Ops:
  0.0 1.4 %copy.21.routes_ref = s32[128,2]{1,0:T(8,128)} copy(s32[128,2]{0,1:T(2,128)} %param.32) | data formatting | bytes 2048 | tf_op args[12]
  1.5 1.4 %copy.22.route_weight_ref = f32[128,2]{1,0:T(8,128)} copy(f32[128,2]{0,1:T(2,128)} %param.33) | data formatting | bytes 2048 | tf_op args[13]
  2.9 0.2 multiply_cosine_fusion
  3.1 0.6 pad_maximum_fusion.table_ref
  3.7 122.6 %shard_map.190 = bf16[128,2048]{1,0:T(8,128)(2,1)} custom-call(bf16[512,128]{1,0:T(8,128)(2,1)} %q_ref.1, bf16[512,128]{1,0:T(8,128)(2,1)} %k_ref.1, bf16[512,256]{1,0:T(8,128)(2,1)} %v_ref.1, f32[512,128]{1,0:T(8,128)} %fwd_ref.1, f32[512,128]{1,0:T(8,128)} %bwd_ref.1, f32[2,72,128]{2,1,0:T(8,128)} %pad_maximum_fusion.table_ref, f32[1,256]{1,0:T(1,128)} %bitcast.7, ...), custom_call_target="tpu_custom_call" | custom-call | tf_op jit(solution)/shard_map/pallas_call | solution.py:706
  126.4 1.9 %copy.24 = bf16[128,2048]{1,0:T(8,128)(2,1)} copy(bf16[128,2048]{1,0:T(8,128)(2,1)} %shard_map.190) | data formatting | bytes 1048576
  (3 shorter events, 0.0 us)

commit v2 on v1

v2 whole, which is shorter than its diff:
```python
import functools

import jax
import jax.numpy as jnp
import numpy as np
from jax import lax
from jax.experimental import pallas as pl
from jax.experimental.pallas import tpu as pltpu
from jax.sharding import PartitionSpec as P

KEY_CHANNELS = 64
DV = 128
BLK = 64
TOPK = 2
ROW_TILE = 16


EPS = 1e-06
GATE_NORM = 16.0
ROPE_BASE = 10000.0
MESH = pl.DeviceIdType.MESH
DEPTH_CUTS = 4
DOWN_CUTS = 8
PIECES_EARLY = 1


def dot_nn(left, right):
    return jnp.dot(left, right, preferred_element_type=jnp.float32)


def dot_nt(left, right):
    return lax.dot_general(
        left, right, (((1,), (1,)), ((), ())), preferred_element_type=jnp.float32
    )


def dot_tn(left, right):
    return lax.dot_general(
        left, right, (((0,), (0,)), ((), ())), preferred_element_type=jnp.float32
    )


def layer_kernel(
    sp_count,
    tp_count,
    capacity,
    return_cuts,
    fwd_hbm,
    bwd_hbm,
    k_hbm,
    v_hbm,
    table_hbm,
    q_hbm,
    out_gate_hbm,
    gain_hbm,
    stream_hbm,
    routes_hbm,
    route_weight_hbm,
    mix_gain_hbm,
    ffn_gain_hbm,
    moe_gain_hbm,
    proj_hbm,
    gate_hbm,
    up_hbm,
    down_hbm,
    shared_gate_hbm,
    shared_up_hbm,
    shared_down_hbm,
    out_ref,
    fwd_ref,
    bwd_ref,
    k_ref,
    v_ref,
    table_ref,
    q_ref,
    out_gate_ref,
    gain_ref,
    stream_ref,
    routes_ref,
    route_weight_ref,
    mix_gain_ref,
    ffn_gain_ref,
    moe_gain_ref,
    proj_ref,
    gate_ref,
    up_ref,
    down_ref,
    sgate_ref,
    sup_ref,
    sdown_ref,
    own_ref,
    got_ref,
    mixed_ref,
    land_ref,
    within_ref,
    key_ref,
    sums_f,
    sums_b,
    heads_ref,
    wide_ref,
    residual_ref,
    normed_ref,
    outgoing_ref,
    arrived_ref,
    silu_ref,
    hidden_ref,
    done_ref,
    back_ref,
    local_sem,
    sum_send,
    sum_recv,
    row_send,
    row_recv,
    block_send,
    block_recv,
    back_send,
    back_recv,
    weight_sem,
    pair_send,
    pair_recv,
    cross_send,
    cross_recv,
    relay_send,
    relay_recv,
    near_send,
    near_recv,
    slice_send,
    slice_recv,
    spread_send,
    spread_recv,
    last_send,
    last_recv,
):
    span, lanes = q_ref.shape
    width = v_ref.shape[1]
    heads = lanes // KEY_CHANNELS
    blocks = span // BLK
    tokens = span // tp_count
    model = stream_ref.shape[1]
    part_width = gate_hbm.shape[2]
    slots = sp_count * capacity
    cut = model // return_cuts
    depth = model // DEPTH_CUTS
    piece = model // DOWN_CUTS
    sp_me = lax.axis_index("sp")
    tp_me = lax.axis_index("tp")
    ranks = tp_count // 2
    rank = lax.div(tp_me, 2)
    seat = lax.rem(tp_me, 2)
    buddy = (sp_me, tp_me + 1 - 2 * seat)
    team = min(8, sp_count)
    place = lax.rem(sp_me, team)
    team_base = sp_me - place
    drains = []

    def sp_peer(step):
        return (lax.rem(sp_me + step, sp_count), tp_me)

    def tp_peer(step):
        return (sp_me, lax.rem(tp_me + step, tp_count))

    def flip(index, mask):
        result, bit = index, 1
        while bit <= mask:
            if mask & bit:
                result = result + bit * (1 - 2 * lax.rem(lax.div(index, bit), 2))
            bit = 2 * bit
        return result

    def mate(distance):
        return (flip(sp_me, distance), tp_me)

    def cross_tp(step):
        return lax.rem(rank + step, ranks) * 2 + seat

    def remote(source, target, send_sem, recv_sem, device):
        return pltpu.make_async_remote_copy(
            src_ref=source,
            dst_ref=target,
            send_sem=send_sem,
            recv_sem=recv_sem,
            device_id=device,
            device_id_type=MESH,
        )

    def send(source, target, send_sem, recv_sem, device):
        copy = remote(source, target, send_sem, recv_sem, device)
        copy.start()
        return copy

    def wait_bytes(ref, semaphore):
        remote(ref, ref, semaphore, semaphore, buddy).wait_recv()

    def sent_bytes(ref, semaphore):
        drains.append(remote(ref, ref, semaphore, semaphore, buddy))

    def fetch(source, target, semaphore):
        copy = pltpu.make_async_copy(source, target, semaphore)
        copy.start()
        return copy

    barrier = pltpu.get_barrier_semaphore()
    for step in range(1, sp_count):
        pl.semaphore_signal(barrier, inc=1, device_id=sp_peer(step), device_id_type=MESH)
    for step in range(1, tp_count):
        pl.semaphore_signal(barrier, inc=1, device_id=tp_peer(step), device_id_type=MESH)
    inputs = [
        fetch(source, target, local_sem.at[at])
        for at, (source, target) in enumerate(
            (
                (fwd_hbm, fwd_ref),
                (bwd_hbm, bwd_ref),
                (k_hbm, k_ref),
                (v_hbm, v_ref),
                (table_hbm, table_ref),
                (q_hbm, q_ref),
                (out_gate_hbm, out_gate_ref),
                (gain_hbm, gain_ref),
                (stream_hbm, stream_ref),
                (routes_hbm, routes_ref),
                (route_weight_hbm, route_weight_ref),
                (mix_gain_hbm, mix_gain_ref),
                (ffn_gain_hbm, ffn_gain_ref),
                (moe_gain_hbm, moe_gain_ref),
            )
        )
    ]

    pieces = [(kind, at) for kind in range(2) for at in range(DEPTH_CUTS)]
    first_down = len(pieces)
    pieces = pieces + [(2, at) for at in range(DOWN_CUTS)]
    count = len(pieces)
    groups = [(0, 0), (1, 0)] + [(2, at) for at in range(DOWN_CUTS)]

    def group_of(index):
        kind, at = pieces[index]
        return 2 + at if kind == 2 else kind

    def group_source(group):
        kind, at = groups[group]
        if kind < 2:
            return (gate_hbm, up_hbm)[kind].at[0]
        return down_hbm.at[0, :, pl.ds(at * piece, piece)]

    def group_slot(group, owner):
        kind, at = groups[group]
        if kind < 2:
            return (gate_ref, up_ref)[kind].at[owner]
        row = pl.multiple_of(owner * part_width, part_width)
        return down_ref.at[at, pl.ds(row, part_width), :]

    def weight_slot(index, owner):
        kind, at = pieces[index]
        if kind < 2:
            return (gate_ref, up_ref)[kind].at[owner, pl.ds(at * depth, depth), :]
        return group_slot(group_of(index), owner)

    shared_lanes = shared_gate_hbm.shape[1]

    def shared_slot(kind, owner, which=None):
        if kind < 2:
            ref = (sgate_ref, sup_ref)[kind].at[owner]
            size = model // team
        else:
            row = pl.multiple_of(owner * shared_lanes, shared_lanes)
            ref = sdown_ref.at[pl.ds(row, shared_lanes), :]
            size = shared_lanes // team
        if which is None:
            return ref
        return ref.at[pl.ds(pl.multiple_of(which * size, size), size), :]

    def shared_source(kind, which=None):
        ref = (shared_gate_hbm, shared_up_hbm, shared_down_hbm)[kind]
        if which is None:
            return ref
        size = (shared_lanes if kind == 2 else model) // team
        return ref.at[pl.ds(pl.multiple_of(which * size, size), size), :]

    shared_fetches = [
        fetch(shared_source(kind), shared_slot(kind, tp_me), local_sem.at[len(inputs) + kind])
        for kind in range(3)
    ]
    weight_fetches = [
        fetch(group_source(group), group_slot(group, tp_me), weight_sem.at[group])
        for group in range(len(groups))
    ]

    inputs.append(fetch(proj_hbm, proj_ref, local_sem.at[len(inputs) + 3]))

    row = lax.broadcasted_iota(jnp.int32, (BLK, BLK), 0)
    column = lax.broadcasted_iota(jnp.int32, (BLK, BLK), 1)
    lower = row >= column
    upper = row <= column
    lower_ones = lower.astype(jnp.bfloat16)
    upper_ones = upper.astype(jnp.bfloat16)
    from_lane = lax.broadcasted_iota(jnp.int32, (lanes, lanes), 0)
    to_lane = lax.broadcasted_iota(jnp.int32, (lanes, lanes), 1)
    half = KEY_CHANNELS // 2
    partner = jnp.where(lax.rem(to_lane, KEY_CHANNELS) < half, to_lane + half, to_lane - half)
    swap = (from_lane == partner).astype(jnp.bfloat16)
    own_head = (
        lax.broadcasted_iota(jnp.int32, (width, lanes), 0) // DV
        == lax.broadcasted_iota(jnp.int32, (width, lanes), 1) // KEY_CHANNELS
    )
    lane_head = lax.broadcasted_iota(jnp.int32, (BLK, lanes), 1) // KEY_CHANNELS

    def rotated(tensor, block):
        at = pl.ds(BLK + sp_me * blocks + block, 1)
        cos_at, sin_at = table_ref[0, at, :], table_ref[1, at, :]
        cos_row, sin_row = table_ref[0, 0:BLK, :], table_ref[1, 0:BLK, :]
        cosine = cos_row * cos_at - sin_row * sin_at
        sine = sin_row * cos_at + cos_row * sin_at
        return tensor.astype(jnp.float32) * cosine + dot_nn(tensor, swap) * sine

    def running(ones, raw):
        logs = (jnp.minimum(raw, 0.0) - jnp.log1p(jnp.exp(-jnp.abs(raw)))) * (1.0 / GATE_NORM)
        first = logs.astype(jnp.bfloat16)
        rest = logs - first.astype(jnp.float32)
        second = rest.astype(jnp.bfloat16)
        third = (rest - second.astype(jnp.float32)).astype(jnp.bfloat16)
        return dot_nn(ones, first) + (dot_nn(ones, second) + dot_nn(ones, third))

    pl.semaphore_wait(barrier, sp_count - 1 + tp_count - 1)

    near, slices = [], []
    for kind in range(3):
        for step in range(1, ranks):
            slices.append(
                send(
                    shared_source(kind, place),
                    shared_slot(kind, tp_me, place),
                    slice_send.at[step - 1, kind],
                    slice_recv.at[step - 1, kind],
                    (sp_me, cross_tp(step)),
                )
            )

    crossings = {}
    whole = (gate_hbm.at[0], up_hbm.at[0], down_hbm.at[0])

    fetched = set()

    def cross(index):
        kind, group = pieces[index][0], group_of(index)
        if group not in fetched:
            fetched.add(group)
            weight_fetches[group].wait()
        crossings[index] = [
            send(
                weight_slot(index, tp_me),
                weight_slot(index, tp_me),
                cross_send.at[step - 1, kind],
                cross_recv.at[step - 1, index],
                (sp_me, cross_tp(step)),
            )
            for step in range(1, ranks)
        ]

    def relay(index):
        kind = pieces[index][0]
        for step in range(1, ranks):
            crossings[index][step - 1].wait_recv()
            owner = lax.rem(rank + ranks - step, ranks) * 2 + seat
            send(
                weight_slot(index, owner),
                weight_slot(index, owner),
                relay_send.at[step - 1, kind],
                relay_recv.at[step - 1, group_of(index)],
                buddy,
            )

    for kind in range(3):
        sent_bytes(whole[kind], pair_send.at[kind])
        for step in range(1, ranks):
            sent_bytes(whole[kind], cross_send.at[step - 1, kind])
            sent_bytes(whole[kind], relay_send.at[step - 1, kind])

    for index in range(PIECES_EARLY):
        cross(index)
    for kind in range(3):
        near.append(
            send(
                shared_source(kind),
                shared_slot(kind, tp_me),
                near_send.at[kind],
                near_recv.at[kind],
                buddy,
            )
        )
    pairs = [
        send(
            group_slot(group, tp_me) if group in fetched else group_source(group),
            group_slot(group, tp_me),
            pair_send.at[groups[group][0]],
            pair_recv.at[group],
            buddy,
        )
        for group in range(len(groups))
    ]

    for copy in inputs[:5]:
        copy.wait()
    cumul_f, cumul_b, decay_f, decay_b = [], [], [], []
    for block in range(blocks):
        rows = pl.ds(block * BLK, BLK)
        total_f = running(lower_ones, fwd_ref[rows, :])
        total_b = running(upper_ones, bwd_ref[rows, :])
        last_f = total_f[BLK - 1 : BLK]
        last_b = total_b[0:1]
        keys = rotated(k_ref[rows, :], block)
        key_ref[rows, :] = keys
        value_rows = v_ref[rows, :]
        out_f = (keys * jnp.exp(last_f - total_f)).astype(jnp.bfloat16)
        out_b = (keys * jnp.exp(last_b - total_b)).astype(jnp.bfloat16)
        sums_f[block] = jnp.where(own_head, dot_tn(value_rows, out_f), 0.0)
        sums_b[block] = jnp.where(own_head, dot_tn(value_rows, out_b), 0.0)
        cumul_f.append(total_f)
        cumul_b.append(total_b)
        decay_f.append(jnp.exp(last_f))
        decay_b.append(jnp.exp(last_b))

    def packed(total):
        return sum(total[h * DV : (h + 1) * DV] for h in range(heads))

    total = sums_f[0]
    through = decay_f[0]
    for block in range(1, blocks):
        total = total * decay_f[block] + sums_f[block]
        through = through * decay_f[block]
    own_ref[0, 0:DV, :] = packed(total).astype(jnp.bfloat16)
    own_ref[0, DV : DV + 16, :] = jnp.broadcast_to(through, (16, lanes)).astype(jnp.bfloat16)
    total = sums_b[blocks - 1]
    through = decay_b[blocks - 1]
    for block in range(blocks - 2, -1, -1):
        total = total * decay_b[block] + sums_b[block]
        through = through * decay_b[block]
    own_ref[1, 0:DV, :] = packed(total).astype(jnp.bfloat16)
    own_ref[1, DV : DV + 16, :] = jnp.broadcast_to(through, (16, lanes)).astype(jnp.bfloat16)

    for step in range(1, sp_count):
        send(
            own_ref.at[lax.div(sp_me + step, sp_count)],
            got_ref.at[step],
            sum_send.at[0],
            sum_recv.at[0],
            sp_peer(step),
        )
    others = pl.ds(1, sp_count - 1)
    sent_bytes(got_ref.at[others], sum_send.at[0])
    inputs[5].wait()
    query_f, query_b = [], []
    for block in range(blocks):
        rows = pl.ds(block * BLK, BLK)
        queries = rotated(q_ref[rows, :], block) * KEY_CHANNELS ** (-0.5)
        keys = key_ref[rows, :]
        total_f, total_b = cumul_f[block], cumul_b[block]
        middle_f = total_f[BLK // 2 - 1 : BLK // 2]
        middle_b = total_b[BLK // 2 : BLK // 2 + 1]
        scaled_qf = queries * jnp.exp(total_f - middle_f)
        scaled_qb = queries * jnp.exp(total_b - middle_b)
        scaled_kf = (keys * jnp.exp(middle_f - total_f)).astype(jnp.bfloat16)
        scaled_kb = (keys * jnp.exp(middle_b - total_b)).astype(jnp.bfloat16)
        query_f.append((queries * jnp.exp(total_f)).astype(jnp.bfloat16))
        query_b.append((queries * jnp.exp(total_b)).astype(jnp.bfloat16))
        for h in range(heads):
            mine = lane_head == h
            scores_f = dot_nt(jnp.where(mine, scaled_qf, 0.0).astype(jnp.bfloat16), scaled_kf)
            scores_b = dot_nt(jnp.where(mine, scaled_qb, 0.0).astype(jnp.bfloat16), scaled_kb)
            scores = jnp.where(lower, scores_f, 0.0) + jnp.where(upper, scores_b, 0.0)
            within_ref[rows, h * DV : (h + 1) * DV] = dot_nn(
                scores.astype(jnp.bfloat16), v_ref[rows, h * DV : (h + 1) * DV]
            )
    wait_bytes(got_ref.at[others], sum_recv.at[0])
    carry_f = jnp.zeros((DV, lanes), jnp.float32)
    carry_b = jnp.zeros((DV, lanes), jnp.float32)
    for step in range(sp_count - 1, 0, -1):
        state = got_ref[step, 0:DV, :].astype(jnp.float32)
        through = got_ref[step, DV : DV + 16, :].astype(jnp.float32)[0:1]
        carry_f = jnp.where(step <= sp_me, carry_f * through + state, carry_f)
    for step in range(1, sp_count):
        state = got_ref[step, 0:DV, :].astype(jnp.float32)
        through = got_ref[step, DV : DV + 16, :].astype(jnp.float32)[0:1]
        carry_b = jnp.where(step > sp_me, carry_b * through + state, carry_b)

    def unpacked(carry):
        return jnp.where(own_head, jnp.concatenate([carry] * heads, axis=0), 0.0)

    state = unpacked(carry_f)
    for block in range(blocks):
        rows = pl.ds(block * BLK, BLK)
        within_ref[rows, :] += dot_nt(query_f[block], state.astype(jnp.bfloat16))
        if block < blocks - 1:
            state = state * decay_f[block] + sums_f[block]
    inputs[6].wait()
    inputs[7].wait()
    state = unpacked(carry_b)
    for block in range(blocks - 1, -1, -1):
        rows = pl.ds(block * BLK, BLK)
        attended = within_ref[rows, :] + dot_nt(query_b[block], state.astype(jnp.bfloat16))
        if block > 0:
            state = state * decay_b[block] + sums_b[block]
        for h in range(heads):
            part = attended[:, h * DV : (h + 1) * DV]
            square = jnp.mean(part * part, axis=-1, keepdims=True)
            gate = out_gate_ref[rows, h * DV : (h + 1) * DV].astype(jnp.float32)
            mixed_ref[rows, h * DV : (h + 1) * DV] = (
                part
                * lax.rsqrt(square + EPS)
                * gain_ref[:, h * DV : (h + 1) * DV]
                * (gate / (1.0 + jnp.exp(-gate)))
            ).astype(jnp.bfloat16)

    row_copies = []
    for step in range(1, tp_count):
        target = lax.rem(tp_me + step, tp_count)
        row_copies.append(
            send(
                mixed_ref.at[pl.ds(pl.multiple_of(target * tokens, tokens), tokens)],
                land_ref.at[tp_me],
                row_send.at[0],
                row_recv.at[step],
                (sp_me, target),
            )
        )
    sent_bytes(mixed_ref.at[pl.ds(0, (tp_count - 1) * tokens)], row_send.at[0])
    for index in range(PIECES_EARLY, count):
        cross(index)
    spread_masks = [0]
    spread_copies = slices
    spread_count = 0

    def spread(bit):
        nonlocal spread_masks, spread_copies, spread_count
        for copy in spread_copies:
            copy.wait_recv()
        spread_copies = []
        for mask in spread_masks:
            which = flip(place, mask)
            for step in range(1, ranks):
                owner = lax.rem(rank + ranks - step, ranks) * 2 + seat
                for kind in range(3):
                    spread_copies.append(
                        send(
                            shared_slot(kind, owner, which),
                            shared_slot(kind, owner, which),
                            spread_send.at[step - 1, kind],
                            spread_recv.at[step - 1, spread_count, kind],
                            mate(bit),
                        )
                    )
            spread_count += 1
        spread_masks = spread_masks + [mask + bit for mask in spread_masks]

    stages = [team >> shift for shift in range(1, team.bit_length())]
    spread(stages[0])
    land_ref[tp_me] = mixed_ref[pl.ds(pl.multiple_of(tp_me * tokens, tokens), tokens), :]

    for copy in inputs[8:]:
        copy.wait()
    token_row = lax.broadcasted_iota(jnp.int32, (tokens, tokens), 0)
    token_column = lax.broadcasted_iota(jnp.int32, (tokens, tokens), 1)
    earlier = (token_row < token_column).astype(jnp.bfloat16)
    expert_row = lax.broadcasted_iota(jnp.int32, (max(8, sp_count), tokens), 0)
    choices = [routes_ref[choice : choice + 1, :] for choice in range(TOPK)]
    named = [(chosen == expert_row).astype(jnp.float32) for chosen in choices]
    before = dot_nn(sum(named).astype(jnp.bfloat16), earlier)
    slot_row = lax.broadcasted_iota(jnp.int32, (slots, tokens), 0)
    weights = jnp.zeros((slots, tokens), jnp.float32)
    picked = jnp.zeros((slots, tokens), jnp.float32)
    for choice in range(TOPK):
        slot = jnp.sum(before * named[choice], axis=0, keepdims=True).astype(jnp.int32)
        distance = lax.bitwise_xor(choices[choice], jnp.full((1, tokens), sp_me, jnp.int32))
        hit = slot_row == distance * capacity + slot
        picked = jnp.where(hit, 1.0, picked)
        weights = jnp.where(hit, route_weight_ref[choice : choice + 1, :], weights)
    picked = picked.astype(jnp.bfloat16)
    weights = jnp.transpose(weights)
    weights_high = weights.astype(jnp.bfloat16)
    weights_low = (weights - weights_high.astype(jnp.float32)).astype(jnp.bfloat16)

    for copy in row_copies:
        copy.wait_recv()
    for source in range(tp_count):
        heads_ref[:, source * width : (source + 1) * width] = land_ref[source]
    square = jnp.zeros((tokens, 1), jnp.float32)
    for at in range(0, model, 512):
        part = dot_nn(heads_ref[...], proj_ref[:, at : at + 512])
        wide_ref[:, at : at + 512] = part
        square = square + jnp.sum(part * part, axis=-1, keepdims=True)
    scale = lax.rsqrt(square * (1.0 / model) + EPS)
    square = jnp.zeros((tokens, 1), jnp.float32)
    for at in range(0, model, 512):
        part = (
            stream_ref[:, at : at + 512].astype(jnp.float32)
            + wide_ref[:, at : at + 512] * scale * mix_gain_ref[:, at : at + 512]
        ).astype(jnp.bfloat16)
        residual_ref[:, at : at + 512] = part
        part = part.astype(jnp.float32)
        square = square + jnp.sum(part * part, axis=-1, keepdims=True)
    scale = lax.rsqrt(square * (1.0 / model) + EPS)
    for at in range(0, model, 512):
        part = (
            residual_ref[:, at : at + 512].astype(jnp.float32)
            * scale
            * ffn_gain_ref[:, at : at + 512]
        ).astype(jnp.bfloat16)
        normed_ref[:, at : at + 512] = part
        outgoing_ref[:, :, at : at + 512] = (
            dot_nn(picked, part).astype(jnp.bfloat16).reshape(sp_count, capacity, 512)
        )

    far = sp_count // 2
    order = list(range(far, sp_count)) + list(range(1, far))
    for distance in order:
        send(
            outgoing_ref.at[distance],
            arrived_ref.at[distance],
            block_send.at[0],
            block_recv.at[distance // far],
            mate(distance),
        )
    sent_bytes(outgoing_ref.at[others], block_send.at[0])
    for bit in stages[1:-1]:
        spread(bit)
    arrived_ref[0] = outgoing_ref[0]

    for index in range(PIECES_EARLY):
        relay(index)

    def arrive(group):
        pairs[group].wait_recv()
        for step in range(1, ranks):
            owner = lax.rem(rank + ranks - step, ranks) * 2 + 1 - seat
            wait_bytes(group_slot(group, owner), relay_recv.at[step - 1, group])

    def put_hidden(owner, low, high, values):
        lane = owner * part_width
        hidden_ref[low * capacity : high * capacity, lane : lane + part_width] = values.astype(
            jnp.bfloat16
        )

    middle = first_down // 2
    for index in range(PIECES_EARLY, middle):
        relay(index)
    if len(stages) > 1:
        spread(stages[-1])
    for index in range(middle, first_down - 2):
        relay(index)
    arrive(0)

    def wait_blocks(low, high):
        inner = pl.ds(max(low, 1), high - max(low, 1))
        if high > max(low, 1):
            wait_bytes(arrived_ref.at[inner], block_recv.at[low // far])

    def rows_of(low, high):
        return arrived_ref[low:high].reshape((high - low) * capacity, model)

    per_cut = DOWN_CUTS // return_cuts

    def give_back(part, low, high):
        for at in range(part * per_cut, (part + 1) * per_cut):
            inner = pl.ds((at - part * per_cut) * piece, piece)
            done_ref[part, low:high, :, inner] = (
                dot_nn(hidden_ref[low * capacity : high * capacity, :], down_ref[at])
                .astype(jnp.bfloat16)
                .reshape(high - low, capacity, piece)
            )
        for distance in order:
            if low <= distance < high:
                send(
                    done_ref.at[part, distance],
                    back_ref.at[part, distance],
                    back_send.at[0],
                    back_recv.at[part],
                    mate(distance),
                )

    def down_ready(part):
        for at in range(part * per_cut, (part + 1) * per_cut):
            relay(first_down + at)
            arrive(2 + at)

    wait_blocks(far, sp_count)
    rows = rows_of(far, sp_count)
    for owner in range(tp_count):
        lane = owner * part_width
        silu_ref[:, lane : lane + part_width] = jax.nn.silu(dot_nn(rows, gate_ref[owner]))
    relay(first_down - 2)
    relay(first_down - 1)
    arrive(1)
    for owner in range(tp_count):
        lane = owner * part_width
        values = silu_ref[:, lane : lane + part_width] * dot_nn(rows, up_ref[owner])
        put_hidden(owner, far, sp_count, values)
    down_ready(0)
    give_back(0, far, sp_count)
    wait_blocks(0, far)
    rows = rows_of(0, far)
    for owner in range(tp_count):
        values = jax.nn.silu(dot_nn(rows, gate_ref[owner])) * dot_nn(rows, up_ref[owner])
        put_hidden(owner, 0, far, values)
    give_back(0, 0, far)
    for part in range(1, return_cuts):
        down_ready(part)
        give_back(part, 0, sp_count)
    for part in range(return_cuts):
        back_ref[part, 0] = done_ref[part, 0]
    sent_bytes(done_ref.at[:, others], back_send.at[0])

    for copy in spread_copies:
        copy.wait_recv()
    lasts = []
    for step in range(1, ranks):
        owner = lax.rem(rank + ranks - step, ranks) * 2 + seat
        for kind in range(3):
            lasts.append(
                send(
                    shared_slot(kind, owner),
                    shared_slot(kind, owner),
                    last_send.at[step - 1, kind],
                    last_recv.at[step - 1, kind],
                    buddy,
                )
            )
    for copy in shared_fetches:
        copy.wait()
    for copy in near + lasts:
        copy.wait_recv()
    shared_hidden = jnp.concatenate(
        [
            jax.nn.silu(dot_nn(normed_ref[...], sgate_ref[owner]))
            * dot_nn(normed_ref[...], sup_ref[owner])
            for owner in range(tp_count)
        ],
        axis=1,
    ).astype(jnp.bfloat16)
    for at in range(0, model, 512):
        wide_ref[:, at : at + 512] = dot_nn(shared_hidden, sdown_ref[:, at : at + 512])

    square = jnp.zeros((tokens, 1), jnp.float32)
    for part in range(return_cuts):
        wait_bytes(back_ref.at[part, others], back_recv.at[part])
        back = back_ref[part].reshape(slots, cut)
        inner = pl.ds(part * cut, cut)
        mixture = wide_ref[:, inner] + dot_nn(weights_high, back) + dot_nn(weights_low, back)
        wide_ref[:, inner] = mixture
        square = square + jnp.sum(mixture * mixture, axis=-1, keepdims=True)
    scale = lax.rsqrt(square * (1.0 / model) + EPS)
    for at in range(0, model, 512):
        out_ref[:, at : at + 512] = (
            residual_ref[:, at : at + 512].astype(jnp.float32)
            + wide_ref[:, at : at + 512] * scale * moe_gain_ref[:, at : at + 512]
        ).astype(out_ref.dtype)
    for kind in range(3):
        size = (shared_lanes if kind == 2 else model) // team * (team - 1)
        ref = (sgate_ref, sup_ref, sdown_ref)[kind]
        for step in range(1, ranks):
            if kind == 2:
                sent_bytes(ref.at[pl.ds(0, size), :], spread_send.at[step - 1, kind])
            else:
                sent_bytes(ref.at[0, pl.ds(0, size), :], spread_send.at[step - 1, kind])
    for copy in slices + near + lasts + drains:
        copy.wait_send()


def body(
    stream,
    queries,
    key_rows,
    values,
    out_gate,
    fwd_decay,
    bwd_decay,
    head_gain,
    out_proj,
    mix_gain,
    ffn_gain,
    moe_gain,
    routes,
    route_weight,
    expert_gate,
    expert_up,
    expert_down,
    shared_gate,
    shared_up,
    shared_down,
):
    sp_count = lax.axis_size("sp")
    tp_count = lax.axis_size("tp")
    tokens, model = stream.shape
    span, lanes = queries.shape
    width = values.shape[1]
    blocks = span // BLK
    part_width = expert_gate.shape[2]
    shared_width = shared_gate.shape[1] * tp_count
    capacity = max(2, 3 * tokens * TOPK // (2 * sp_count))
    capacity = -(-capacity // ROW_TILE) * ROW_TILE
    slots = sp_count * capacity
    return_cuts = DOWN_CUTS if sp_count <= 16 else 1
    team = min(8, sp_count)
    ranks = tp_count // 2

    half = KEY_CHANNELS // 2
    lane = np.arange(lanes) % KEY_CHANNELS
    frequency = ROPE_BASE ** (-(lane % half) / half)
    positions = np.concatenate([np.arange(BLK), np.arange(sp_count * blocks) * BLK])
    angles = positions[:, None] * frequency[None, :]
    sign = np.where(lane < half, -1.0, 1.0)
    table = jnp.asarray(np.stack([np.cos(angles), np.sin(angles) * sign]), jnp.float32)

    vmem = pl.BlockSpec(memory_space=pltpu.VMEM)
    hbm = pl.BlockSpec(memory_space=pl.ANY)
    dma = pltpu.SemaphoreType.DMA
    bf16, f32 = jnp.bfloat16, jnp.float32
    count = 2 * DEPTH_CUTS + DOWN_CUTS
    groups = 2 + DOWN_CUTS
    inputs = (
        fwd_decay,
        bwd_decay,
        key_rows,
        values,
        table,
        queries,
        out_gate,
        head_gain.reshape(1, -1),
        stream,
        routes.T,
        route_weight.T,
        mix_gain.reshape(1, -1),
        ffn_gain.reshape(1, -1),
        moe_gain.reshape(1, -1),
        out_proj,
    )
    updated = pl.pallas_call(
        functools.partial(layer_kernel, sp_count, tp_count, capacity, return_cuts),
        out_shape=jax.ShapeDtypeStruct(stream.shape, bf16),
        in_specs=[hbm] * (len(inputs) + 6),
        out_specs=vmem,
        scratch_shapes=[
            *(pltpu.VMEM(array.shape, array.dtype) for array in inputs),
            pltpu.VMEM((tp_count, model, part_width), bf16),
            pltpu.VMEM((tp_count, model, part_width), bf16),
            pltpu.VMEM((DOWN_CUTS, tp_count * part_width, model // DOWN_CUTS), bf16),
            pltpu.VMEM((tp_count, model, shared_width // tp_count), bf16),
            pltpu.VMEM((tp_count, model, shared_width // tp_count), bf16),
            pltpu.VMEM((shared_width, model), bf16),
            pltpu.VMEM((2, DV + 16, lanes), bf16),
            pltpu.VMEM((sp_count, DV + 16, lanes), bf16),
            pltpu.VMEM((span, width), bf16),
            pltpu.VMEM((tp_count, tokens, width), bf16),
            pltpu.VMEM((span, width), f32),
            pltpu.VMEM((span, lanes), f32),
            pltpu.VMEM((blocks, width, lanes), f32),
            pltpu.VMEM((blocks, width, lanes), f32),
            pltpu.VMEM((tokens, tp_count * width), bf16),
            pltpu.VMEM((tokens, model), f32),
            pltpu.VMEM((tokens, model), bf16),
            pltpu.VMEM((tokens, model), bf16),
            pltpu.VMEM((sp_count, capacity, model), bf16),
            pltpu.VMEM((sp_count, capacity, model), bf16),
            pltpu.VMEM((slots // 2, tp_count * part_width), f32),
            pltpu.VMEM((slots, tp_count * part_width), bf16),
            pltpu.VMEM((return_cuts, sp_count, capacity, model // return_cuts), bf16),
            pltpu.VMEM((return_cuts, sp_count, capacity, model // return_cuts), bf16),
            dma((len(inputs) + 3,)),
            dma((1,)),
            dma((1,)),
            dma((1,)),
            dma((tp_count,)),
            dma((1,)),
            dma((2,)),
            dma((1,)),
            dma((return_cuts,)),
            dma((groups,)),
            dma((3,)),
            dma((groups,)),
            dma((ranks - 1, 3)),
            dma((ranks - 1, count)),
            dma((ranks - 1, 3)),
            dma((ranks - 1, groups)),
            dma((3,)),
            dma((3,)),
            dma((ranks - 1, 3)),
            dma((ranks - 1, 3)),
            dma((ranks - 1, 3)),
            dma((ranks - 1, team - 1, 3)),
            dma((ranks - 1, 3)),
            dma((ranks - 1, 3)),
        ],
        compiler_params=pltpu.CompilerParams(
            collective_id=0, has_side_effects=True, vmem_limit_bytes=62 * 2**20
        ),
    )(
        *inputs,
        expert_gate,
        expert_up,
        expert_down,
        shared_gate,
        shared_up,
        shared_down,
    )
    return updated


def solution(mesh):
    return jax.shard_map(
        body,
        mesh=mesh,
        in_specs=(
            P(("sp", "tp"), None),
            P("sp", "tp"),
            P("sp", "tp"),
            P("sp", "tp"),
            P("sp", "tp"),
            P("sp", "tp"),
            P("sp", "tp"),
            P("tp"),
            P(),
            P(),
            P(),
            P(),
            P(("sp", "tp"), None),
            P(("sp", "tp"), None),
            P("sp", None, "tp"),
            P("sp", None, "tp"),
            P("sp", "tp", None),
            P(None, "tp"),
            P(None, "tp"),
            P("tp", None),
        ),
        out_specs=P(("sp", "tp"), None),
        check_vma=False,
    )
```

time: 129 us -> 105 us (0.81)
  Pallas kernels: 123 us -> 103 us
  local copies, waits for them, and re-layouts: 4.72 us -> 1.88 us
    pallas_call x1, Pallas kernels: 123 us -> 103 us  [body(): pl.pallas_call(functools.partial(layer_kernel, sp_count, tp_count, capaci...]
    unnamed x3 -> x1, local copies, waits for them, and re-layouts: 4.72 us -> 1.88 us
where the time goes in v2:
time: 105 us
  Pallas kernels  103 us (98%)
  local copies, waits for them, and re-layouts  1.88 us (2%)
    pallas_call x1, Pallas kernels, body(): pl.pallas_call(functools.partial(layer_kernel, sp_count, tp_count, capaci...  103 us

profile of v2, /device:TPU:0, one launch (start us, length us, event | category | flops | bytes accessed | tf_op | source)
XLA Modules:
  0.0 104.9 jit_solution(14134233414229275156)
XLA Ops:
  0.0 103.1 %shard_map.199 = bf16[128,2048]{1,0:T(8,128)(2,1)} custom-call(f32[512,128]{1,0:T(8,128)} %fwd_hbm.1, f32[512,128]{1,0:T(8,128)} %bwd_hbm.1, bf16[512,128]{1,0:T(8,128)(2,1)} %k_hbm.1, bf16[512,256]{1,0:T(8,128)(2,1)} %v_hbm.1, f32[2,128,128]{2,1,0:T(8,128)} %constant.2.clone.table_hbm, bf16[512,128]{1,0:T(8,128)(2,1)} %q_hbm.1, ...), custom_call_target="tpu_custom_call" | custom-call | tf_op jit(solution)/shard_map/pallas_call | solution.py:835
  103.1 1.9 %copy.23 = bf16[128,2048]{1,0:T(8,128)(2,1)} copy(bf16[128,2048]{1,0:T(8,128)(2,1)} %shard_map.199) | data formatting | bytes 1048576

commit v3 on v2

--- a/solution.py
+++ b/solution.py
@@ -19,8 +19,8 @@
 GATE_NORM = 16.0
 ROPE_BASE = 10000.0
 MESH = pl.DeviceIdType.MESH
-DEPTH_CUTS = 4
-DOWN_CUTS = 8
+DEPTH_UNITS = ((1, 1, 2), (2, 1, 1))
+DOWN_UNITS = (2, 3, 4, 4, 3)
 PIECES_EARLY = 1
 
 
@@ -139,9 +139,8 @@
     model = stream_ref.shape[1]
     part_width = gate_hbm.shape[2]
     slots = sp_count * capacity
-    cut = model // return_cuts
-    depth = model // DEPTH_CUTS
-    piece = model // DOWN_CUTS
+    unit = model // sum(DOWN_UNITS)
+    depth = model // sum(DEPTH_UNITS[0])
     sp_me = lax.axis_index("sp")
     tp_me = lax.axis_index("tp")
     ranks = tp_count // 2
@@ -226,11 +225,16 @@
         )
     ]
 
-    pieces = [(kind, at) for kind in range(2) for at in range(DEPTH_CUTS)]
+    pieces = [(kind, at) for kind in range(2) for at in range(len(DEPTH_UNITS[kind]))]
     first_down = len(pieces)
-    pieces = pieces + [(2, at) for at in range(DOWN_CUTS)]
+    pieces = pieces + [(2, at) for at in range(len(DOWN_UNITS))]
     count = len(pieces)
-    groups = [(0, 0), (1, 0)] + [(2, at) for at in range(DOWN_CUTS)]
+    groups = [(0, 0), (1, 0)] + [(2, at) for at in range(len(DOWN_UNITS))]
+
+    def columns(first, last, origin=0):
+        start = sum(DOWN_UNITS[origin:first]) * unit
+        return pl.ds(start, sum(DOWN_UNITS[first:last]) * unit)
+
 
     def group_of(index):
         kind, at = pieces[index]
@@ -240,19 +244,21 @@
         kind, at = groups[group]
         if kind < 2:
             return (gate_hbm, up_hbm)[kind].at[0]
-        return down_hbm.at[0, :, pl.ds(at * piece, piece)]
+        return down_hbm.at[0, :, columns(at, at + 1)]
 
     def group_slot(group, owner):
         kind, at = groups[group]
         if kind < 2:
             return (gate_ref, up_ref)[kind].at[owner]
         row = pl.multiple_of(owner * part_width, part_width)
-        return down_ref.at[at, pl.ds(row, part_width), :]
+        return down_ref[at].at[pl.ds(row, part_width), :]
 
     def weight_slot(index, owner):
         kind, at = pieces[index]
         if kind < 2:
-            return (gate_ref, up_ref)[kind].at[owner, pl.ds(at * depth, depth), :]
+            units = DEPTH_UNITS[kind]
+            rows = pl.ds(sum(units[:at]) * depth, units[at] * depth)
+            return (gate_ref, up_ref)[kind].at[owner, rows, :]
         return group_slot(group_of(index), owner)
 
     shared_lanes = shared_gate_hbm.shape[1]
@@ -377,27 +383,6 @@
 
     for index in range(PIECES_EARLY):
         cross(index)
-    for kind in range(3):
-        near.append(
-            send(
-                shared_source(kind),
-                shared_slot(kind, tp_me),
-                near_send.at[kind],
-                near_recv.at[kind],
-                buddy,
-            )
-        )
-    pairs = [
-        send(
-            group_slot(group, tp_me) if group in fetched else group_source(group),
-            group_slot(group, tp_me),
-            pair_send.at[groups[group][0]],
-            pair_recv.at[group],
-            buddy,
-        )
-        for group in range(len(groups))
-    ]
-
     for copy in inputs[:5]:
         copy.wait()
     cumul_f, cumul_b, decay_f, decay_b = [], [], [], []
@@ -623,6 +608,27 @@
     for bit in stages[1:-1]:
         spread(bit)
     arrived_ref[0] = outgoing_ref[0]
+    for kind in range(3):
+        near.append(
+            send(
+                shared_source(kind),
+                shared_slot(kind, tp_me),
+                near_send.at[kind],
+                near_recv.at[kind],
+                buddy,
+            )
+        )
+    pairs = [
+        send(
+            group_slot(group, tp_me) if group in fetched else group_source(group),
+            group_slot(group, tp_me),
+            pair_send.at[groups[group][0]],
+            pair_recv.at[group],
+            buddy,
+        )
+        for group in range(len(groups))
+    ]
+
 
     for index in range(PIECES_EARLY):
         relay(index)
@@ -656,21 +662,21 @@
     def rows_of(low, high):
         return arrived_ref[low:high].reshape((high - low) * capacity, model)
 
-    per_cut = DOWN_CUTS // return_cuts
+    per_cut = len(DOWN_UNITS) // return_cuts
 
     def give_back(part, low, high):
         for at in range(part * per_cut, (part + 1) * per_cut):
-            inner = pl.ds((at - part * per_cut) * piece, piece)
-            done_ref[part, low:high, :, inner] = (
-                dot_nn(hidden_ref[low * capacity : high * capacity, :], down_ref[at])
+            inner = columns(at, at + 1, part * per_cut)
+            done_ref[part][low:high, :, inner] = (
+                dot_nn(hidden_ref[low * capacity : high * capacity, :], down_ref[at][...])
                 .astype(jnp.bfloat16)
-                .reshape(high - low, capacity, piece)
+                .reshape(high - low, capacity, inner.size)
             )
         for distance in order:
             if low <= distance < high:
                 send(
-                    done_ref.at[part, distance],
-                    back_ref.at[part, distance],
+                    done_ref[part].at[distance],
+                    back_ref[part].at[distance],
                     back_send.at[0],
                     back_recv.at[part],
                     mate(distance),
@@ -705,8 +711,8 @@
         down_ready(part)
         give_back(part, 0, sp_count)
     for part in range(return_cuts):
-        back_ref[part, 0] = done_ref[part, 0]
-    sent_bytes(done_ref.at[:, others], back_send.at[0])
+        back_ref[part][0] = done_ref[part][0]
+    sent_bytes(outgoing_ref.at[others], back_send.at[0])
 
     for copy in spread_copies:
         copy.wait_recv()
@@ -740,9 +746,9 @@
 
     square = jnp.zeros((tokens, 1), jnp.float32)
     for part in range(return_cuts):
-        wait_bytes(back_ref.at[part, others], back_recv.at[part])
-        back = back_ref[part].reshape(slots, cut)
-        inner = pl.ds(part * cut, cut)
+        wait_bytes(back_ref[part].at[others], back_recv.at[part])
+        inner = columns(part * per_cut, (part + 1) * per_cut)
+        back = back_ref[part][...].reshape(slots, inner.size)
         mixture = wide_ref[:, inner] + dot_nn(weights_high, back) + dot_nn(weights_low, back)
         wide_ref[:, inner] = mixture
         square = square + jnp.sum(mixture * mixture, axis=-1, keepdims=True)
@@ -797,7 +803,10 @@
     capacity = max(2, 3 * tokens * TOPK // (2 * sp_count))
     capacity = -(-capacity // ROW_TILE) * ROW_TILE
     slots = sp_count * capacity
-    return_cuts = DOWN_CUTS if sp_count <= 16 else 1
+    return_cuts = len(DOWN_UNITS) if sp_count <= 16 else 1
+    unit = model // sum(DOWN_UNITS)
+    cuts = [width * unit for width in DOWN_UNITS]
+    back_cuts = cuts if return_cuts > 1 else [model]
     team = min(8, sp_count)
     ranks = tp_count // 2
 
@@ -813,8 +822,8 @@
     hbm = pl.BlockSpec(memory_space=pl.ANY)
     dma = pltpu.SemaphoreType.DMA
     bf16, f32 = jnp.bfloat16, jnp.float32
-    count = 2 * DEPTH_CUTS + DOWN_CUTS
-    groups = 2 + DOWN_CUTS
+    count = sum(len(units) for units in DEPTH_UNITS) + len(DOWN_UNITS)
+    groups = 2 + len(DOWN_UNITS)
     inputs = (
         fwd_decay,
         bwd_decay,
@@ -841,7 +850,7 @@
             *(pltpu.VMEM(array.shape, array.dtype) for array in inputs),
             pltpu.VMEM((tp_count, model, part_width), bf16),
             pltpu.VMEM((tp_count, model, part_width), bf16),
-            pltpu.VMEM((DOWN_CUTS, tp_count * part_width, model // DOWN_CUTS), bf16),
+            [pltpu.VMEM((tp_count * part_width, cut), bf16) for cut in cuts],
             pltpu.VMEM((tp_count, model, shared_width // tp_count), bf16),
             pltpu.VMEM((tp_count, model, shared_width // tp_count), bf16),
             pltpu.VMEM((shared_width, model), bf16),
@@ -861,8 +870,8 @@
             pltpu.VMEM((sp_count, capacity, model), bf16),
             pltpu.VMEM((slots // 2, tp_count * part_width), f32),
             pltpu.VMEM((slots, tp_count * part_width), bf16),
-            pltpu.VMEM((return_cuts, sp_count, capacity, model // return_cuts), bf16),
-            pltpu.VMEM((return_cuts, sp_count, capacity, model // return_cuts), bf16),
+            [pltpu.VMEM((sp_count, capacity, cut), bf16) for cut in back_cuts],
+            [pltpu.VMEM((sp_count, capacity, cut), bf16) for cut in back_cuts],
             dma((len(inputs) + 3,)),
             dma((1,)),
             dma((1,)),

time: 105 us -> 104 us (level)
  no operation moved by 1% of the time
where the time goes in v3:
time: 104 us
  Pallas kernels  102 us (98%)
  local copies, waits for them, and re-layouts  1.88 us (2%)
    pallas_call x1, Pallas kernels, body(): pl.pallas_call(functools.partial(layer_kernel, sp_count, tp_count, capaci...  102 us

profile of v3, /device:TPU:0, one launch (start us, length us, event | category | flops | bytes accessed | tf_op | source)
XLA Modules:
  0.0 104.0 jit_solution(12065205154807592383)
XLA Ops:
  0.0 102.1 %shard_map.199 = bf16[128,2048]{1,0:T(8,128)(2,1)} custom-call(f32[512,128]{1,0:T(8,128)} %fwd_hbm.1, f32[512,128]{1,0:T(8,128)} %bwd_hbm.1, bf16[512,128]{1,0:T(8,128)(2,1)} %k_hbm.1, bf16[512,256]{1,0:T(8,128)(2,1)} %v_hbm.1, f32[2,128,128]{2,1,0:T(8,128)} %constant.2.clone.table_hbm, bf16[512,128]{1,0:T(8,128)(2,1)} %q_hbm.1, ...), custom_call_target="tpu_custom_call" | custom-call | tf_op jit(solution)/shard_map/pallas_call | solution.py:844
  102.1 1.9 %copy.23 = bf16[128,2048]{1,0:T(8,128)(2,1)} copy(bf16[128,2048]{1,0:T(8,128)(2,1)} %shard_map.199) | data formatting | bytes 1048576
